TPU v7x, 256 devices: a whole 4x4x8 slice. The times are simulated.
256 devices in a mesh: sp: 64 (over z, y, core), tp: 4 (over x).
Axes of the slice: x: 4, y: 4, z: 8, core: 2. Of those that a mesh axis runs over, the one named last changes fastest.
Arguments:
- moe_input: bfloat16 [8192, 2048], P('sp', 'tp'), may hold values from -6 to 6
- cotangent: bfloat16 [8192, 2048], P('sp', 'tp'), may hold values from -16 to 16
- expert_ids: int32 [8192, 2], P('sp'), may hold values from 0 to 63, as said below
- routing_weights: float32 [8192, 2], P('sp'), may hold values from 0.1 to 0.6
- gate_weight: bfloat16 [64, 2048, 1024], P('sp', None, 'tp'), may hold values from -0.125 to 0.125
- up_weight: bfloat16 [64, 2048, 1024], P('sp', None, 'tp'), may hold values from -0.125 to 0.125
- down_weight: bfloat16 [64, 1024, 2048], P('sp', 'tp'), may hold values from -0.1875 to 0.1875
- inner_x: bfloat16 [8192, 4096], P('sp', 'tp'), may hold values from -6 to 6
- inner_b: bfloat16 [8192, 256], P('sp', 'tp'), may hold values from -6 to 6
- inner_c: bfloat16 [8192, 256], P('sp', 'tp'), may hold values from -6 to 6
- gate_z: bfloat16 [8192, 4096], P('sp', 'tp'), may hold values from -6 to 6
- step_raw: float32 [8192, 64], P('sp', 'tp'), may hold values from -30 to 2
- decay_rate: float32 [64], P('tp'), may hold values from 1 to 16
- skip_weight: float32 [64], P('tp'), may hold values from 0.1 to 1.9
- norm_gain: float32 [4096], P('tp'), may hold values from 0.1 to 1.9
- w_out: bfloat16 [2048, 4096], P(None, 'tp'), may hold values from -0.09375 to 0.09375
Outputs:
- gate_weight_gradient: bfloat16 [64, 2048, 1024], P('sp', None, 'tp')
- up_weight_gradient: bfloat16 [64, 2048, 1024], P('sp', None, 'tp')
- down_weight_gradient: bfloat16 [64, 1024, 2048], P('sp', 'tp')
- grad_out: float32 [2048, 4096], P('sp', 'tp')
- grad_inner_x: bfloat16 [8192, 4096], P('sp', 'tp')
- grad_inner_b: float32 [8192, 256], P('sp', 'tp')
- grad_inner_c: float32 [8192, 256], P('sp', 'tp')
- grad_gate_z: bfloat16 [8192, 4096], P('sp', 'tp')
- grad_step_raw: float32 [8192, 64], P('sp', 'tp')
Inputs may be any that keep to these rules, and one draw needn't show every extreme that they name: `expert_ids`: the two entries of a row differ and lie in the same group of 16 consecutive experts. In each aligned block of 128 rows no expert is named more than 8 times; one group of experts, the same for all blocks, takes exactly half of every block's rows, and each of its experts is named exactly 8 times in every block.
All inputs are finite; a program needn't handle non-finite values.
Results may differ from a plain program's by a relative error of at most 0.015.
Values may be sent and summed in bfloat16 or wider, within the bound.
A program may use at most 128 MiB of HBM per device.

v0:
```python
from functools import partial

import jax
import jax.numpy as jnp
from jax import lax
from jax.sharding import Mesh
from jax.sharding import PartitionSpec as P

HEAD_DIM = 64
STATE = 64
SPAN = 128
SP = ("sp_0", "sp_1", "sp_2")


EPS = 0.01


def sent_together(arrays, axis, split_dim, concat_dim, along):
    both = jnp.concatenate(arrays, axis=along)
    out, at, finished = (
        lax.all_to_all(both, axis, split_axis=split_dim, concat_axis=concat_dim, tiled=True),
        0,
        [],
    )
    for a in arrays:
        finished.append(lax.slice_in_dim(out, at, at + a.shape[along], axis=along))
        at += a.shape[along]
    return tuple(finished)


def in_one_piece(arrays, axis, dim, along):
    both = jnp.concatenate(arrays, axis=along)
    out, at, finished = (lax.all_gather(both, axis, axis=dim, tiled=True), 0, [])
    for a in arrays:
        finished.append(lax.slice_in_dim(out, at, at + a.shape[along], axis=along))
        at += a.shape[along]
    return tuple(finished)


def cut_along(shard, dim, devices):
    before, after = (shard.shape[:dim], shard.shape[dim + 1 :])
    return jnp.moveaxis(shard.reshape(*before, devices, -1, *after), dim, 0)


def sum_at_owner(shard, axis, dim):
    devices = lax.axis_size(axis)
    tiles = lax.all_to_all(cut_along(shard, dim, devices), axis, 0, 0, tiled=True)
    return jnp.sum(tiles.astype(jnp.float32), axis=0)


def from_everyone(shard, axis):
    copies = jnp.broadcast_to(shard, (lax.axis_size(axis), *shard.shape))
    return lax.all_to_all(copies, axis, split_axis=0, concat_axis=0, tiled=True)


def in_order(tiles, dim):
    tiles = jnp.moveaxis(tiles, 0, dim)
    dims = tiles.shape
    return tiles.reshape(*dims[:dim], dims[dim] * dims[dim + 1], *dims[dim + 2 :])


def gathered_copies(shard, axis, dim):
    tiles = from_everyone(shard, axis)
    return in_order(tiles, dim)


def neutral_like(shard, identity):
    return jax.tree.map(
        lambda a, e: jnp.broadcast_to(jnp.asarray(e, a.dtype), a.shape), shard, identity
    )


def prefix_by_axis(shard, axes, combine, identity):
    before = start = neutral_like(shard, identity)
    subtotal = shard
    for axis in reversed(axes):
        devices, mine = (lax.axis_size(axis), lax.axis_index(axis))
        pieces = jax.tree.map(
            lambda part, kind: lax.all_gather(part.astype(kind), axis),
            subtotal,
            (jnp.bfloat16, jnp.bfloat16),
        )
        inside, subtotal = (start, start)
        for k in range(devices):
            passed = k < mine
            subtotal = combine(
                subtotal, jax.tree.map(lambda part, own: part[k].astype(own.dtype), pieces, shard)
            )
            inside = jax.tree.map(lambda new, old: jnp.where(passed, new, old), subtotal, inside)
        before = combine(inside, before)
    return before


def own_rows(subtotal, axes):
    for axis in axes:
        subtotal = lax.psum_scatter(subtotal, axis, scatter_dimension=0, tiled=True)
    return subtotal


def carried_in(shard, axes, combine, identity):
    before = start = neutral_like(shard, identity)
    subtotal = shard
    for axis in reversed(axes):
        devices, mine = (lax.axis_size(axis), lax.axis_index(axis))
        pieces = jax.tree.map(
            lambda part, kind: lax.all_gather(part.astype(kind), axis),
            subtotal,
            jax.tree.map(lambda a: jnp.bfloat16 if a.dtype == jnp.float32 else a.dtype, shard),
        )
        inside, subtotal = (start, start)
        for k in reversed(range(devices)):
            passed = k > mine
            subtotal = combine(
                subtotal, jax.tree.map(lambda part, own: part[k].astype(own.dtype), pieces, shard)
            )
            inside = jax.tree.map(lambda new, old: jnp.where(passed, new, old), subtotal, inside)
        before = combine(inside, before)
    return before


def slot_positions(chosen, expert_list, expert_capacity):
    listed = chosen.reshape(-1)
    onehot = (listed[:, None] == jnp.arange(expert_list, dtype=jnp.int32)[None, :]).astype(
        jnp.int32
    )
    before = jnp.cumsum(onehot, axis=0) - onehot
    return listed * expert_capacity + jnp.sum(before * onehot, axis=1)


def prepare(inner_x32, inner_b32, step_raw, decays):
    tok_rows = inner_x32.shape[0]
    heads = decays.shape[0]
    groups = inner_b32.shape[1] // STATE
    per_group = heads // groups
    blocks = tok_rows // SPAN
    x_act = jax.nn.silu(inner_x32).reshape(tok_rows, heads, HEAD_DIM)
    b_blocks = jax.nn.silu(inner_b32).reshape(blocks, SPAN, groups, STATE)
    step_size = jax.nn.softplus(step_raw)
    decay_log = (-step_size * decays[None, :]).reshape(blocks, SPAN, groups, per_group)
    scaled = (x_act * step_size[:, :, None]).reshape(blocks, SPAN, groups, per_group, HEAD_DIM)
    return (x_act, b_blocks, decay_log, scaled)


def advance(carry_state, block_in):
    x_block, log_block, b_block = block_in
    running = jnp.cumsum(log_block, axis=0)
    to_end = jnp.exp(running[-1] - running)
    fresh_state = jnp.einsum("lgn,lge,lgep->gepn", b_block, to_end, x_block)
    return (carry_state * jnp.exp(running[-1])[:, :, None, None] + fresh_state, None)


def block_outputs(carry_state, block_in):
    x_block, log_block, b_block, c_block = block_in
    span_len = x_block.shape[0]
    running = jnp.cumsum(log_block, axis=0)
    places = jnp.arange(span_len)
    causal = (places[:, None] >= places[None, :])[:, :, None, None]
    between = running[:, None] - running[None, :]
    weights = jnp.where(causal, jnp.exp(jnp.where(causal, between, 0.0)), 0.0)
    scores = jnp.einsum("lgn,sgn->lsg", c_block, b_block)
    inside = jnp.einsum("lsg,lsge,sgep->lgep", scores, weights, x_block)
    carried = jnp.einsum("lgn,gepn,lge->lgep", c_block, carry_state, jnp.exp(running))
    to_end = jnp.exp(running[-1] - running)
    fresh_state = jnp.einsum("lgn,lge,lgep->gepn", b_block, to_end, x_block)
    return (carry_state * jnp.exp(running[-1])[:, :, None, None] + fresh_state, inside + carried)


def mixer_output(
    inner_x32, inner_b32, inner_c32, gate_z32, step_raw, carry_in, decays, skip_weight, norm_gain
):
    tok_rows = inner_x32.shape[0]
    heads = decays.shape[0]
    groups = inner_b32.shape[1] // STATE
    x_act, b_blocks, decay_log, scaled = prepare(inner_x32, inner_b32, step_raw, decays)
    c_blocks = jax.nn.silu(inner_c32).reshape(tok_rows // SPAN, SPAN, groups, STATE)
    outputs = lax.scan(block_outputs, carry_in, (scaled, decay_log, b_blocks, c_blocks))[1]
    mixed_out = outputs.reshape(tok_rows, heads, HEAD_DIM) + x_act * skip_weight[None, :, None]
    gated_out = mixed_out.reshape(tok_rows, heads * HEAD_DIM) * jax.nn.silu(gate_z32)
    grouped = gated_out.reshape(tok_rows, groups, -1)
    normed = grouped * lax.rsqrt(jnp.mean(grouped * grouped, axis=2, keepdims=True) + EPS)
    return normed.reshape(tok_rows, -1) * norm_gain[None, :]


def carry_forward(earlier, latter):
    return (earlier[0] * latter[0], earlier[1] * latter[0][:, :, None, None] + latter[1])


def carry_back(earlier, latter):
    return (latter[0] * earlier[0], latter[1] + latter[0][:, :, None, None] * earlier[1])


def body(
    moe_input,
    cotangent,
    expert_ids,
    routing_weights,
    gate_weight,
    up_weight,
    down_weight,
    inner_x,
    inner_b,
    inner_c,
    gate_z,
    step_raw,
    decay_rate,
    skip_weight,
    norm_gain,
    w_out,
):
    tok_rows, chosen_count = expert_ids.shape
    local_experts = gate_weight.shape[0]
    senders = lax.axis_size(SP)
    expert_list = local_experts * senders
    expert_capacity = 4 * tok_rows // expert_list
    place_into_slots = slot_positions(expert_ids, expert_list, expert_capacity)
    owner = (
        jnp.full((expert_list * expert_capacity,), tok_rows, jnp.int32)
        .at[place_into_slots]
        .set(jnp.arange(tok_rows * chosen_count, dtype=jnp.int32) // chosen_count)
    )
    scaling = (
        jnp.zeros((expert_list * expert_capacity,), jnp.float32)
        .at[place_into_slots]
        .set(routing_weights.reshape(-1))
    )

    def to_slots(source, weighted):
        padded = jnp.concatenate([source, jnp.zeros((1, source.shape[1]), source.dtype)], axis=0)
        picked = padded[owner]
        if weighted:
            picked = (picked.astype(jnp.float32) * scaling[:, None]).astype(jnp.bfloat16)
        return picked.reshape(senders, local_experts, expert_capacity, source.shape[1])

    part_in, part_grad = sent_together(
        (to_slots(moe_input, False), to_slots(cotangent, True)), SP, 0, 0, 1
    )
    routed_in, routed_grad = in_one_piece((part_in, part_grad), "tp", 3, 0)
    gate_pre = jnp.einsum(
        "secd,edf->secf", routed_in, gate_weight, preferred_element_type=jnp.float32
    )
    up_pre = jnp.einsum("secd,edf->secf", routed_in, up_weight, preferred_element_type=jnp.float32)
    sigmoid_gate = jax.nn.sigmoid(gate_pre)
    active = gate_pre * sigmoid_gate
    hidden = (active * up_pre).astype(jnp.bfloat16)
    hidden_grad = jnp.einsum(
        "secd,efd->secf", routed_grad, down_weight, preferred_element_type=jnp.float32
    )
    gate_grad = (
        hidden_grad * up_pre * sigmoid_gate * (1.0 + gate_pre * (1.0 - sigmoid_gate))
    ).astype(jnp.bfloat16)
    up_grad = (hidden_grad * active).astype(jnp.bfloat16)
    slot_terms = jnp.einsum(
        "secf,edf->secd", gate_grad, gate_weight, preferred_element_type=jnp.float32
    )
    slot_terms = slot_terms + jnp.einsum(
        "secf,edf->secd", up_grad, up_weight, preferred_element_type=jnp.float32
    )
    summed = sum_at_owner(slot_terms.astype(jnp.bfloat16), "tp", 3).astype(jnp.bfloat16)
    returned = lax.all_to_all(summed, SP, split_axis=0, concat_axis=0, tiled=True)
    down_weight_gradient = jnp.einsum(
        "secf,secd->efd", hidden, routed_grad, preferred_element_type=jnp.float32
    ).astype(jnp.bfloat16)
    gate_weight_gradient = jnp.einsum(
        "secd,secf->edf", routed_in, gate_grad, preferred_element_type=jnp.float32
    ).astype(jnp.bfloat16)
    up_weight_gradient = jnp.einsum(
        "secd,secf->edf", routed_in, up_grad, preferred_element_type=jnp.float32
    ).astype(jnp.bfloat16)
    back_rows = returned.reshape(expert_list * expert_capacity, returned.shape[3])
    moe_grad = jnp.sum(
        back_rows[place_into_slots].astype(jnp.float32).reshape(tok_rows, chosen_count, -1), axis=1
    )
    mixer_cols = (cotangent.astype(jnp.float32) + moe_grad).astype(jnp.bfloat16)
    mixer_rows = gathered_copies(mixer_cols, "tp", 1)
    inner_x32 = inner_x.astype(jnp.float32)
    inner_b32 = inner_b.astype(jnp.float32)

    def local_states(x_in, b_in, raw_in):
        x_act, b_blocks, decay_log, scaled = prepare(x_in, b_in, raw_in, decay_rate)
        totals = jnp.exp(jnp.sum(decay_log, axis=(0, 1)))
        initial = jnp.zeros((decay_log.shape[2], decay_log.shape[3], HEAD_DIM, STATE), jnp.float32)
        return (totals, lax.scan(advance, initial, (scaled, decay_log, b_blocks))[0])

    (totals, fresh), states_pull = jax.vjp(local_states, inner_x32, inner_b32, step_raw)
    identity = (jnp.ones_like(totals), jnp.zeros_like(fresh))
    carry_in = prefix_by_axis((totals, fresh), SP, carry_forward, identity)[1]
    output_fn = partial(
        mixer_output, decays=decay_rate, skip_weight=skip_weight, norm_gain=norm_gain
    )
    normed, output_pull = jax.vjp(
        output_fn,
        inner_x32,
        inner_b32,
        inner_c.astype(jnp.float32),
        gate_z.astype(jnp.float32),
        step_raw,
        carry_in,
    )
    norm_rows = normed.astype(jnp.bfloat16)
    grad_out = own_rows(
        lax.dot_general(
            mixer_rows, norm_rows, (((0,), (0,)), ((), ())), preferred_element_type=jnp.float32
        ),
        SP,
    )
    norm_grad = jnp.dot(mixer_rows, w_out, preferred_element_type=jnp.float32)
    x_grad_out, b_grad_out, c_grad, z_grad, raw_grad_out, state_grad = output_pull(norm_grad)
    after_grad = carried_in((totals, state_grad), SP, carry_back, identity)[1]
    x_grad_state, b_grad_state, raw_grad_state = states_pull(
        (jnp.sum(after_grad * carry_in, axis=(2, 3)), after_grad)
    )
    grad_inner_x = (x_grad_out + x_grad_state).astype(jnp.bfloat16)
    grad_inner_b = b_grad_out + b_grad_state
    grad_step_raw = raw_grad_out + raw_grad_state
    return (
        gate_weight_gradient,
        up_weight_gradient,
        down_weight_gradient,
        grad_out,
        grad_inner_x,
        grad_inner_b,
        c_grad,
        z_grad.astype(jnp.bfloat16),
        grad_step_raw,
    )


def solution(mesh):
    finer = Mesh(mesh.devices.reshape(8, 4, 2, mesh.shape["tp"]), ("sp_0", "sp_1", "sp_2", "tp"))
    return jax.shard_map(
        body,
        mesh=finer,
        in_specs=(
            P(SP, "tp"),
            P(SP, "tp"),
            P(SP, None),
            P(SP, None),
            P(SP, None, "tp"),
            P(SP, None, "tp"),
            P(SP, "tp", None),
            P(SP, "tp"),
            P(SP, "tp"),
            P(SP, "tp"),
            P(SP, "tp"),
            P(SP, "tp"),
            P("tp"),
            P("tp"),
            P("tp"),
            P(None, "tp"),
        ),
        out_specs=(
            P(SP, None, "tp"),
            P(SP, None, "tp"),
            P(SP, "tp", None),
            P(SP, "tp"),
            P(SP, "tp"),
            P(SP, "tp"),
            P(SP, "tp"),
            P(SP, "tp"),
            P(SP, "tp"),
        ),
        check_vma=False,
    )
```

profile of v0, /device:TPU:1, one launch (start us, length us, event | category | flops | bytes accessed | tf_op | source)
XLA Modules:
  0.0 419.9 jit_solution(6886294324005378016)
XLA Ops:
  11.2 1.4 scatter_custom_fusion
  13.5 1.4 scatter_custom_fusion.1
  16.9 2.0 gather_fusion.1
  18.8 2.0 gather_fusion
  21.1 41.1 %all_to_all.20 = bf16[64,2,8,512]{3,2,1,0:T(8,128)(2,1)S(1)} all-to-all(bf16[64,2,8,512]{3,2,1,0:T(8,128)(2,1)S(1)} %pad_maximum_fusion), channel_id=1, replica_groups=mesh['sp_0'=8,'sp_1'=4,'sp_2'=2,'tp'=4] {'sp_0','sp_1','sp_2'}, dimensions={0} | all-to-all | bytes 2097152 | tf_op jit(solution)/shard_map/all_to_all | solution.py:21
  65.1 3.3 all-reduce.6
  68.5 7.6 %all_gather.53 = bf16[4,1,16]{2,1,0:T(2,128)(2,1)S(1)} all-gather(bf16[1,1,16]{2,1,0:T(2,128)(2,1)S(1)} %convert_bitcast_fusion.44), channel_id=1, replica_groups=mesh['sp_0'=8,'sp_1'=4,'sp_2'=2,'tp'=4] {'sp_1'}, dimensions={0}, use_global_device_ids=true | all-gather | bytes 160 | tf_op jit(solution)/shard_map/all_gather | solution.py:79
  77.3 4.2 all-gather.1
  82.3 28.8 %all-gather.7.cloned.1.call-done = bf16[128,1,8,2048]{3,2,0,1:T(8,128)(2,1)} async-done(((bf16[128,1,8,512]{3,2,0,1:T(8,128)(2,1)}), bf16[128,1,8,2048]{3,2,0,1:T(8,128)(2,1)}) %all-gather.7.cloned.1.call-update) | async-done | bytes 4194320 | tf_op jit(solution)/shard_map/all_gather | solution.py:33
  111.1 2.5 fusion.10
  113.5 2.5 fusion.9
  119.0 1.5 copy.178
  120.5 4.5 %all-to-all-start.1 = ((bf16[4,64,1,8,512]{4,3,1,2,0:T(8,128)(2,1)}), bf16[4,64,1,8,512]{4,3,1,2,0:T(8,128)(2,1)}, u32[]{:S(2)}, u32[]{:S(2)}) async-start(bf16[4,64,1,8,512]{4,3,1,2,0:T(8,128)(2,1)} %bitcast.960), calls=%async_computation.1 | async-start | bytes 4194304 | tf_op jit(solution)/shard_map/all_to_all | solution.py:47
  126.1 13.7 %all_gather.57 = bf16[4,1,16,64,64]{4,3,2,1,0:T(8,128)(2,1)S(1)} all-gather(bf16[1,1,16,64,64]{4,3,2,1,0:T(8,128)(2,1)S(1)} %fusion.251), channel_id=1, replica_groups=mesh['sp_0'=8,'sp_1'=4,'sp_2'=2,'tp'=4] {'sp_1'}, dimensions={0}, use_global_device_ids=true | all-gather | bytes 655360 | tf_op jit(solution)/shard_map/all_gather | solution.py:79
  142.9 7.7 %all-to-all-done.1 = bf16[4,64,1,8,512]{4,3,1,2,0:T(8,128)(2,1)} async-done(((bf16[4,64,1,8,512]{4,3,1,2,0:T(8,128)(2,1)}), bf16[4,64,1,8,512]{4,3,1,2,0:T(8,128)(2,1)}, u32[]{:S(2)}, u32[]{:S(2)}) %all-to-all-start.1) | async-done | bytes 2097184 | tf_op jit(solution)/shard_map/all_to_all | solution.py:47
  150.6 2.9 reduce_sum.194
  153.4 11.7 %all-to-all-start.2 = ((bf16[64,1,8,512]{3,2,1,0:T(8,128)(2,1)}), bf16[64,1,8,512]{3,2,1,0:T(8,128)(2,1)S(1)}, u32[]{:S(2)}, u32[]{:S(2)}) async-start(bf16[64,1,8,512]{3,2,1,0:T(8,128)(2,1)} %bitcast.45), calls=%async_computation.2 | async-start | bytes 1048576 | tf_op jit(solution)/shard_map/all_to_all | solution.py:259
  167.3 25.6 %all_gather.54 = bf16[8,1,16]{2,1,0:T(2,128)(2,1)S(1)} all-gather(bf16[1,1,16]{2,1,0:T(2,128)(2,1)S(1)} %get-tuple-element.407), channel_id=1, replica_groups=mesh['sp_0'=8,'sp_1'=4,'sp_2'=2,'tp'=4] {'sp_0'}, dimensions={0}, use_global_device_ids=true | all-gather | bytes 288 | tf_op jit(solution)/shard_map/all_gather | solution.py:79
  194.7 1.2 gather_fusion.2
  197.9 3.5 all-to-all-start.3
  201.5 3.0 convolution_bitcast_fusion.7
  205.5 2.7 all-to-all-done.3
  208.3 3.5 multiply_reduce_fusion.8
  211.9 1.2 fusion.149
  214.9 5.4 %all-gather.2 = bf16[32,64,64]{2,1,0:T(8,128)(2,1)S(1)} all-gather(bf16[16,64,64]{2,1,0:T(8,128)(2,1)S(1)} %fusion.15), channel_id=4, replica_groups=mesh['sp_0'=8,'sp_1'=4,'sp_2'=2,'tp'=4] {'sp_2'}, dimensions={0}, use_global_device_ids=true | all-gather | bytes 393216 | tf_op jit(solution)/shard_map/all_gather | solution.py:106
  220.5 13.2 %all_gather.61 = bf16[4,1,16,64,64]{4,3,2,1,0:T(8,128)(2,1)S(1)} all-gather(bf16[1,1,16,64,64]{4,3,2,1,0:T(8,128)(2,1)S(1)} %fusion.257), channel_id=1, replica_groups=mesh['sp_0'=8,'sp_1'=4,'sp_2'=2,'tp'=4] {'sp_1'}, dimensions={0}, use_global_device_ids=true | all-gather | bytes 655360 | tf_op jit(solution)/shard_map/all_gather | solution.py:106
  235.0 5.8 %fusion.261 = f32[2048,1024]{1,0:T(8,128)} fusion(bf16[128,2048]{0,1:T(8,128)(2,1)} %bitcast.967, f32[128,1024]{1,0:T(8,128)} %copy-done.13, f32[1024]{0:T(1024)S(1)} %copy-done.68, f32[128]{0:T(128)S(1)} %copy-done.59), kind=kOutput, calls=%fused_computation.373 | convolution fusion | flops 537264128 | bytes 9441792 | tf_op jit(solution)/shard_map/dot_general | solution.py:301
  243.0 2.0 copy.131
  245.0 11.9 %all_gather.63 = bf16[8,1,16]{2,1,0:T(2,128)(2,1)S(1)} all-gather(bf16[1,1,16]{2,1,0:T(2,128)(2,1)S(1)} %copy-done.81), channel_id=1, replica_groups=mesh['sp_0'=8,'sp_1'=4,'sp_2'=2,'tp'=4] {'sp_0'}, dimensions={0}, use_global_device_ids=true | all-gather | bytes 288 | tf_op jit(solution)/shard_map/all_gather | solution.py:106
  260.0 3.7 fusion.4
  263.7 1.9 fusion.5
  265.7 1.8 fusion.3
  267.5 1.4 fusion.40
  269.7 1.3 multiply_reduce_fusion.2
  272.5 2.5 fusion.12
  275.0 2.1 copy.130
  277.1 1.5 fusion.17
  278.7 3.2 convolution_bitcast_fusion.10
  282.7 3.3 fusion.71
  286.0 2.5 multiply_reduce_fusion.1
  288.5 1.4 copy.171
  289.9 1.4 copy.160
  291.3 79.3 %reduce-scatter.4.cloned.1.call-done = f32[256,1024]{1,0:T(8,128)} async-done(((f32[2048,1024]{1,0:T(8,128)}), f32[256,1024]{1,0:T(8,128)}) %reduce-scatter.4.cloned.1.call-update) | async-done | bytes 1048592 | tf_op jit(solution)/shard_map/reduce_scatter | solution.py:96
  371.1 5.8 %multiply_reduce_fusion.4 = (f32[16]{0:T(128)}, f32[16]{0:T(128)S(1)}, f32[16]{0:T(128)}) fusion(pred[]{:T(512)S(6)} %lt.80, pred[]{:T(512)S(6)} %lt.79, pred[]{:T(512)S(6)} %lt.78, pred[]{:T(512)S(6)} %lt.77, pred[]{:T(512)S(6)} %lt.76, pred[]{:T(512)S(6)} %lt.75, pred[]{:T(512)S(6)} %lt.74, f32[16]{0:T(128)} %fusion.411, ...), kind=kLoop, calls=%fused_computation.321 | loop fusion | flops 7864272 | bytes 3672156 | tf_op jit(solution)/shard_map/reduce_sum | solution.py:310
  383.8 2.1 copy.133
  385.9 8.5 %reduce-scatter.6.cloned.1.call-done = f32[64,1024]{1,0:T(8,128)} async-done(((f32[256,1024]{1,0:T(8,128)}), f32[64,1024]{1,0:T(8,128)}) %reduce-scatter.6.cloned.1.call-update) | async-done | bytes 262160 | tf_op jit(solution)/shard_map/reduce_scatter | solution.py:96
  395.4 2.3 fusion.208
  397.6 15.0 %reduce-scatter.8.cloned.1.call-done = f32[32,1024]{1,0:T(8,128)} async-done(((f32[64,1024]{1,0:T(8,128)}), f32[32,1024]{1,0:T(8,128)}) %reduce-scatter.8.cloned.1.call-update) | async-done | bytes 131088 | tf_op jit(solution)/shard_map/reduce_scatter | solution.py:96
  (302 shorter events, 43.8 us)
Async XLA Ops:
  8.0 103.0 %copy-start = (bf16[1,2048,256]{2,1,0:T(8,128)(2,1)S(1)}, bf16[1,2048,256]{2,1,0:T(8,128)(2,1)}, u32[]{:S(2)}) copy-start(bf16[1,2048,256]{2,1,0:T(8,128)(2,1)} %param.21) | copy-start | bytes 3145732
  8.0 103.0 %all-gather.7.cloned.1.call-start = ((), (), s32[]{:S(2)}) async-start(), calls=%async_computation.7 | async-start | bytes 5242880 | tf_op jit(solution)/shard_map/all_gather | solution.py:33
  62.3 14.1 %copy-start.8 = (bf16[128,1024]{1,0:T(8,128)(2,1)S(1)}, bf16[128,1024]{1,0:T(8,128)(2,1)}, u32[]{:S(2)}) copy-start(bf16[128,1024]{1,0:T(8,128)(2,1)} %param.24) | copy-start | bytes 786436
  63.4 13.4 %copy-start.19 = (bf16[128,64]{0,1:T(8,128)(2,1)S(1)}, bf16[128,64]{0,1:T(8,128)(2,1)}, u32[]{:S(2)}) copy-start(bf16[128,64]{0,1:T(8,128)(2,1)} %param.25) | copy-start | bytes 49156
  63.5 12.9 %copy-start.15 = (f32[128,16]{1,0:T(8,128)}, f32[128,16]{1,0:T(8,128)S(1)}, u32[]{:S(2)}) copy-start(f32[128,16]{1,0:T(8,128)S(1)} %copy.116) | copy-start | bytes 24580
  64.9 11.6 %copy-start.83 = (f32[16]{0:T(128)}, f32[16]{0:T(128)S(1)}, u32[]{:S(2)}) copy-start(f32[16]{0:T(128)S(1)} %get-tuple-element.371) | copy-start | bytes 196
  68.4 56.6 %copy-start.42 = (bf16[32]{0:T(256)(128)(2,1)}, bf16[32]{0:T(256)(128)(2,1)S(1)}, u32[]{:S(2)}) copy-start(bf16[32]{0:T(256)(128)(2,1)S(1)} %all-reduce.6) | copy-start | bytes 196
  76.1 63.7 %copy-start.32 = (bf16[4,1,16]{2,1,0:T(2,128)(2,1)}, bf16[4,1,16]{2,1,0:T(2,128)(2,1)S(1)}, u32[]{:S(2)}) copy-start(bf16[4,1,16]{2,1,0:T(2,128)(2,1)S(1)} %all_gather.53) | copy-start | bytes 388
  81.5 119.9 %copy-start.2 = (bf16[32,64,64]{2,1,0:T(8,128)(2,1)}, bf16[32,64,64]{2,1,0:T(8,128)(2,1)S(1)}, u32[]{:S(2)}) copy-start(bf16[32,64,64]{2,1,0:T(8,128)(2,1)S(1)} %all-gather.1) | copy-start | bytes 786436
  82.3 43.3 %copy-start.64 = (f32[16]{0:T(128)}, f32[16]{0:T(128)S(1)}, u32[]{:S(2)}) copy-start(f32[16]{0:T(128)S(1)} %get-tuple-element.409) | copy-start | bytes 196
  82.3 58.1 %copy-start.60 = (f32[16]{0:T(128)}, f32[16]{0:T(128)S(1)}, u32[]{:S(2)}) copy-start(f32[16]{0:T(128)S(1)} %get-tuple-element.403) | copy-start | bytes 196
  120.5 30.1 %all-to-all-start.1 = ((bf16[4,64,1,8,512]{4,3,1,2,0:T(8,128)(2,1)}), bf16[4,64,1,8,512]{4,3,1,2,0:T(8,128)(2,1)}, u32[]{:S(2)}, u32[]{:S(2)}) async-start(bf16[4,64,1,8,512]{4,3,1,2,0:T(8,128)(2,1)} %bitcast.960), calls=%async_computation.1 | async-start | bytes 4194304 | tf_op jit(solution)/shard_map/all_to_all | solution.py:47
  124.9 17.2 %copy-start.85 = (f32[16]{0:T(128)S(1)}, f32[16]{0:T(128)}, u32[]{:S(2)}) copy-start(f32[16]{0:T(128)} %param.30) | copy-start | bytes 196
  124.9 76.5 %all-gather.9.cloned.1.call-start = ((), (), s32[]{:S(2)}) async-start(), calls=%async_computation.8 | async-start | bytes 2359296 | tf_op jit(solution)/shard_map/all_gather | solution.py:79
  140.4 13.1 %copy-start.50 = (f32[16]{0:T(128)}, f32[16]{0:T(128)S(1)}, u32[]{:S(2)}) copy-start(f32[16]{0:T(128)S(1)} %get-tuple-element.401) | copy-start | bytes 196
  140.4 13.1 %copy-start.62 = (f32[16]{0:T(128)}, f32[16]{0:T(128)S(1)}, u32[]{:S(2)}) copy-start(f32[16]{0:T(128)S(1)} %get-tuple-element.399) | copy-start | bytes 196
  141.4 23.7 %copy-start.44 = (bf16[128,64]{0,1:T(8,128)(2,1)S(1)}, bf16[128,64]{0,1:T(8,128)(2,1)}, u32[]{:S(2)}) copy-start(bf16[128,64]{0,1:T(8,128)(2,1)} %param.26) | copy-start | bytes 49156
  142.2 24.6 %copy-start.33 = (bf16[4,1,16]{2,1,0:T(2,128)(2,1)S(1)}, bf16[4,1,16]{2,1,0:T(2,128)(2,1)}, u32[]{:S(2)}) copy-start(bf16[4,1,16]{2,1,0:T(2,128)(2,1)} %copy-done.32) | copy-start | bytes 388
  142.2 50.7 %copy-start.70 = (s32[256,1]{0,1:T(1,128)S(1)}, s32[256,1]{0,1:T(1,128)}, u32[]{:S(2)}) copy-start(s32[256,1]{0,1:T(1,128)} %copy-done.69) | copy-start | bytes 3076
  153.4 41.3 %all-to-all-start.2 = ((bf16[64,1,8,512]{3,2,1,0:T(8,128)(2,1)}), bf16[64,1,8,512]{3,2,1,0:T(8,128)(2,1)S(1)}, u32[]{:S(2)}, u32[]{:S(2)}) async-start(bf16[64,1,8,512]{3,2,1,0:T(8,128)(2,1)} %bitcast.45), calls=%async_computation.2 | async-start | bytes 1048576 | tf_op jit(solution)/shard_map/all_to_all | solution.py:259
  165.4 31.5 %copy-start.18 = (bf16[128,512]{1,0:T(8,128)(2,1)S(1)}, bf16[128,512]{1,0:T(8,128)(2,1)}, u32[]{:S(2)}) copy-start(bf16[128,512]{1,0:T(8,128)(2,1)} %param.18) | copy-start | bytes 393220
  197.9 10.4 %all-to-all-start.3 = ((bf16[4,128,512]{1,2,0:T(8,128)(2,1)}), bf16[4,128,512]{1,2,0:T(8,128)(2,1)S(1)}, u32[]{:S(2)}, u32[]{:S(2)}) async-start(bf16[4,128,512]{1,2,0:T(8,128)(2,1)} %broadcast_in_dim.198), calls=%async_computation.3 | async-start | bytes 1048576 | tf_op jit(solution)/shard_map/all_to_all | solution.py:53
  201.3 81.3 %all-gather.11.cloned.1.call-start = ((), (), s32[]{:S(2)}) async-start(), calls=%async_computation.12 | async-start | bytes 2359296 | tf_op jit(solution)/shard_map/all_gather | solution.py:106
  213.3 20.5 %copy-start.49 = (f32[16]{0:T(128)S(1)}, f32[16]{0:T(128)}, u32[]{:S(2)}) copy-start(f32[16]{0:T(128)} %copy-done.48) | copy-start | bytes 196
  213.3 20.4 %copy-start.51 = (f32[16]{0:T(128)S(1)}, f32[16]{0:T(128)}, u32[]{:S(2)}) copy-start(f32[16]{0:T(128)} %copy-done.50) | copy-start | bytes 196
  213.4 20.4 %copy-start.52 = (f32[16]{0:T(128)S(1)}, f32[16]{0:T(128)}, u32[]{:S(2)}) copy-start(f32[16]{0:T(128)} %get-tuple-element.402) | copy-start | bytes 196
  213.4 20.4 %copy-start.53 = (f32[16]{0:T(128)S(1)}, f32[16]{0:T(128)}, u32[]{:S(2)}) copy-start(f32[16]{0:T(128)} %get-tuple-element.398) | copy-start | bytes 196
  214.8 20.1 %copy-start.59 = (f32[128]{0:T(128)S(1)}, f32[128]{0:T(128)}, u32[]{:S(2)}) copy-start(f32[128]{0:T(128)} %copy-done.58) | copy-start | bytes 1540
  214.9 20.1 %copy-start.68 = (f32[1024]{0:T(1024)S(1)}, f32[1024]{0:T(1024)}, u32[]{:S(2)}) copy-start(f32[1024]{0:T(1024)} %param.31) | copy-start | bytes 12292
  234.9 135.8 %reduce-scatter.4.cloned.1.call-start = ((), (), s32[]{:S(2)}) async-start(), calls=%async_computation.9 | async-start | bytes 9437184 | tf_op jit(solution)/shard_map/reduce_scatter | solution.py:96
  240.8 16.8 %copy-start.34 = (bf16[4,1,16]{2,1,0:T(2,128)(2,1)S(1)}, bf16[4,1,16]{2,1,0:T(2,128)(2,1)}, u32[]{:S(2)}) copy-start(bf16[4,1,16]{2,1,0:T(2,128)(2,1)} %copy-done.32) | copy-start | bytes 388
  240.8 16.8 %copy-start.43 = (bf16[32]{0:T(256)(128)(2,1)S(1)}, bf16[32]{0:T(256)(128)(2,1)}, u32[]{:S(2)}) copy-start(bf16[32]{0:T(256)(128)(2,1)} %copy-done.42) | copy-start | bytes 196
  240.8 18.0 %copy-start.20 = (bf16[128,64]{0,1:T(8,128)(2,1)S(1)}, bf16[128,64]{0,1:T(8,128)(2,1)}, u32[]{:S(2)}) copy-start(bf16[128,64]{0,1:T(8,128)(2,1)} %param.25) | copy-start | bytes 49156
  240.8 153.6 %reduce-scatter.6.cloned.1.call-start = ((), (), s32[]{:S(2)}) async-start(), calls=%async_computation.10 | async-start | bytes 1310720 | tf_op jit(solution)/shard_map/reduce_scatter | solution.py:96
  269.6 9.0 %copy-start.65 = (f32[16]{0:T(128)S(1)}, f32[16]{0:T(128)}, u32[]{:S(2)}) copy-start(f32[16]{0:T(128)} %copy-done.64) | copy-start | bytes 196
  269.6 9.0 %copy-start.67 = (f32[16]{0:T(128)S(1)}, f32[16]{0:T(128)}, u32[]{:S(2)}) copy-start(f32[16]{0:T(128)} %copy-done.66) | copy-start | bytes 196
  269.6 9.0 %copy-start.72 = (f32[16]{0:T(128)S(1)}, f32[16]{0:T(128)}, u32[]{:S(2)}) copy-start(f32[16]{0:T(128)} %get-tuple-element.391) | copy-start | bytes 196
  269.6 9.0 %copy-start.73 = (f32[16]{0:T(128)S(1)}, f32[16]{0:T(128)}, u32[]{:S(2)}) copy-start(f32[16]{0:T(128)} %get-tuple-element.392) | copy-start | bytes 196
  269.6 9.0 %copy-start.74 = (f32[16]{0:T(128)S(1)}, f32[16]{0:T(128)}, u32[]{:S(2)}) copy-start(f32[16]{0:T(128)} %get-tuple-element.393) | copy-start | bytes 196
  269.6 9.0 %copy-start.75 = (f32[16]{0:T(128)S(1)}, f32[16]{0:T(128)}, u32[]{:S(2)}) copy-start(f32[16]{0:T(128)} %get-tuple-element.394) | copy-start | bytes 196
  370.7 41.9 %reduce-scatter.8.cloned.1.call-start = ((), (), s32[]{:S(2)}) async-start(), calls=%async_computation.11 | async-start | bytes 393216 | tf_op jit(solution)/shard_map/reduce_scatter | solution.py:96
  376.8 17.6 %copy-start.21 = (bf16[128,64]{0,1:T(8,128)(2,1)S(1)}, bf16[128,64]{0,1:T(8,128)(2,1)}, u32[]{:S(2)}) copy-start(bf16[128,64]{0,1:T(8,128)(2,1)} %param.25) | copy-start | bytes 49156
  376.8 17.6 %copy-start.37 = (f32[128,64]{0,1:T(8,128)S(1)}, f32[128,64]{0,1:T(8,128)}, u32[]{:S(2)}) copy-start(f32[128,64]{0,1:T(8,128)} %fusion.17) | copy-start | bytes 98308
  376.8 18.5 %copy-start.4 = (f32[128,1024]{1,0:T(8,128)S(1)}, f32[128,1024]{1,0:T(8,128)}, u32[]{:S(2)}) copy-start(f32[128,1024]{1,0:T(8,128)} %copy-done.3) | copy-start | bytes 1572868
  376.8 18.5 %copy-start.9 = (bf16[128,1024]{1,0:T(8,128)(2,1)S(1)}, bf16[128,1024]{1,0:T(8,128)(2,1)}, u32[]{:S(2)}) copy-start(bf16[128,1024]{1,0:T(8,128)(2,1)} %param.24) | copy-start | bytes 786436
  376.8 18.5 %copy-start.10 = (f32[128,1024]{1,0:T(8,128)S(1)}, f32[128,1024]{1,0:T(8,128)}, u32[]{:S(2)}) copy-start(f32[128,1024]{1,0:T(8,128)} %copy.131) | copy-start | bytes 1572868
  376.8 18.5 %copy-start.36 = (f32[1024]{0:T(1024)S(1)}, f32[1024]{0:T(1024)}, u32[]{:S(2)}) copy-start(f32[1024]{0:T(1024)} %mul.1525) | copy-start | bytes 12292
  383.8 28.8 %copy-start.1 = (bf16[1,2048,256]{2,1,0:T(8,128)(2,1)S(1)}, bf16[1,2048,256]{2,1,0:T(8,128)(2,1)}, u32[]{:S(2)}) copy-start(bf16[1,2048,256]{2,1,0:T(8,128)(2,1)} %param.21) | copy-start | bytes 3145732
  (56 other events, 226.8 us)
Sparse Core Ops, SparseCore 0:
  63.5 47.4 all-gather.6
  370.8 23.5 reduce-scatter.5
  397.5 15.0 reduce-scatter.7
Sparse Core Ops, SparseCore 1:
  141.5 50.7 all-gather.8
  235.0 35.6 all-gather.10
  273.0 97.6 reduce-scatter.3
where the time goes:
time: 421 us; the launch traced here: 420 us
  waiting for transfers between devices  142 us (34%)
  blocking collectives  126 us (30%)
  matrix products  42.9 us (10%)
  local copies, waits for them, and re-layouts  37.4 us (9%)
  other arithmetic  33.8 us (8%)
  starting transfers between devices  20.2 us (5%)
  between operations  17.4 us (4%)
    reduce_scatter x3, waiting for transfers between devices, own_rows(): subtotal = lax.psum_scatter(subtotal, axis, scatter_dimension=0, tiled=True)  103 us
    all_gather x4, blocking collectives, prefix_by_axis(): lax.all_gather(part.astype(kind), axis)  51.1 us
    all_to_all x1, blocking collectives, sent_together(): lax.all_to_all(both, axis, split_axis=split_dim, concat_axis=concat_dim,...  41.1 us
    all_gather x3, blocking collectives, carried_in(): lax.all_gather(part.astype(kind), axis)  30.6 us
    all_gather x1, waiting for transfers between devices, in_one_piece(): lax.all_gather(both, axis, axis=dim, tiled=True)  28.8 us
    all_to_all x1, starting transfers between devices, body(): lax.all_to_all(summed, SP, split_axis=0, concat_axis=0, tiled=True)  11.7 us
  transfers between devices with their start and end apart: 9, of which 6 were waited for; matrix products, arithmetic and copies ran while one was open for 19% of the time, Pallas kernels for 0%

commit v1 on v0

v1 whole, which is shorter than its diff:
```python
import jax
import jax.numpy as jnp
from jax import lax
from jax.experimental import pallas as pl
from jax.experimental.pallas import tpu as pltpu
from jax.sharding import Mesh
from jax.sharding import PartitionSpec as P

SP = ("sp_0", "sp_1", "sp_2")

NZ, NY, NC, NX = 8, 4, 2, 4
PEERS = 64
DIMS_TN = (((0,), (0,)), ((), ()))
DIMS_NT = (((1,), (1,)), ((), ()))
DIMS_NN = (((1,), (0,)), ((), ()))
F32 = jnp.float32
BF16 = jnp.bfloat16
MESH = pl.DeviceIdType.MESH


def mm(a, b, dims=DIMS_NN):
    return lax.dot_general(a, b, dims, preferred_element_type=F32)


def plane_at(z, i):
    odd = lax.rem(i, 2)
    off = odd * lax.div(i + 1, 2) + (1 - odd) * (NZ - lax.div(i, 2))
    return lax.rem(z + off, NZ)


def tok_slots(ids):
    e_iota = lax.broadcasted_iota(jnp.int32, (PEERS, 128), 0)
    hot = [(jnp.broadcast_to(ids[k : k + 1, :], (PEERS, 128)) == e_iota).astype(F32) for k in (0, 1)]
    earlier = (
        lax.broadcasted_iota(jnp.int32, (128, 128), 0) < lax.broadcasted_iota(jnp.int32, (128, 128), 1)
    ).astype(BF16)
    counts = mm((hot[0] + hot[1]).astype(BF16), earlier)
    return [
        ids[k : k + 1, :].astype(F32) * 8.0 + jnp.sum(hot[k] * counts, axis=0, keepdims=True)
        for k in (0, 1)
    ]


def to_column(row):
    eye = lax.broadcasted_iota(jnp.int32, (128, 128), 0) == lax.broadcasted_iota(
        jnp.int32, (128, 128), 1
    )
    return jnp.sum(jnp.where(eye, jnp.broadcast_to(row, (128, 128)), 0.0), axis=1, keepdims=True)


EPS = 0.01


def split2(v):
    hi = v.astype(BF16)
    return hi, (v - hi.astype(F32)).astype(BF16)


def spread(v, e):
    hi, lo = split2(v)
    return mm(hi, e) + mm(lo, e)


def per_head(v, e):
    hi, lo = split2(v)
    return mm(hi, e, DIMS_NT) + mm(lo, e, DIMS_NT)


def tri_sum(tri, v):
    hi = v.astype(BF16)
    rest = v - hi.astype(F32)
    mid = rest.astype(BF16)
    lo = (rest - mid.astype(F32)).astype(BF16)
    return mm(tri, hi) + mm(tri, mid) + mm(tri, lo)


def sigmoid(v):
    return 1.0 / (1.0 + jnp.exp(-v))


def iota(shape, dim):
    return lax.broadcasted_iota(jnp.int32, shape, dim)


def head_map():
    return (lax.div(iota((16, 1024), 1), 64) == iota((16, 1024), 0)).astype(F32).astype(BF16)


def two_rows(dec):
    hi = dec.astype(BF16).astype(F32)
    row = iota((16, dec.shape[1]), 0)
    return jnp.where(row == 0, hi, jnp.where(row == 1, dec - hi, 0.0))


def fused_kernel(
    ids_ref, wts_ref, min_ref, cot_ref, ix_ref, ib_ref, ic_ref, gz_ref, raw_ref, decay_ref,
    skip_ref, gain_ref, gw_hbm, uw_hbm, dw_hbm, wo_hbm,
    go_ref, gx_ref, gb_ref, gc_ref, gzz_ref, graw_ref, gwg_hbm, uwg_hbm, dwg_hbm,
    sendbuf, ybuf, gw, uw, dw, own_acc, nbr_acc, rs1_s, rs1_r, rs2_s, rs2_r,
    ggi, hid, retbuf, backbuf, rows, gout, dout,
    w_sem, o_sem, disp_ss, disp_rs, ret_ss, ret_rs,
    a1_s, a1_r, a2_s, a2_r, r1_s, r1_r, r2_s, r2_r, m_s, m_r,
    wo, scaled_ref, stepx_ref, erx_ref, tex_ref, r_ref, rt_ref, scores_ref, w_ref, m_ref,
    inside_ref, carry_ref, carried_ref, nr, gated_ref, inv_ref, dy_ref, ds1_ref, dsc_ref,
    msg_a, rec_a, msg_b, rec_b, msg_c, rec_c, pref, prefd, turned, turned_in, part, parts_in,
    sa_s, sa_r, sb_s, sb_r, sc_s, sc_r, n_s, n_r, t1_s, t1_r, t2_s, t2_r,
):
    z, y, c, x = (lax.axis_index(a) for a in ("sp_0", "sp_1", "sp_2", "tp"))
    sp = z * 8 + y * 2 + c
    me_yc = y * 2 + c
    right, left = lax.rem(x + 1, NX), lax.rem(x + 3, NX)
    far = lax.rem(x + 2, NX)

    def peer(zz, m):
        return {"sp_0": zz, "sp_1": lax.div(m, 2), "sp_2": lax.rem(m, 2)}

    barrier = pltpu.get_barrier_semaphore()

    def greet(i, carry):
        zz, m = lax.div(i, 8), lax.rem(i, 8)

        @pl.when(i != sp)
        def _():
            pl.semaphore_signal(barrier, inc=1, device_id=peer(zz, m), device_id_type=MESH)

        return carry

    lax.fori_loop(0, PEERS, greet, 0)
    for side in (right, left):
        pl.semaphore_signal(barrier, inc=1, device_id={"tp": side}, device_id_type=MESH)

    loads = [
        pltpu.make_async_copy(src, dst, w_sem.at[k])
        for k, (src, dst) in enumerate(((gw_hbm, gw), (uw_hbm, uw), (dw_hbm, dw), (wo_hbm, wo)))
    ]
    for load in loads:
        load.start()

    ids = ids_ref[...]
    wts = wts_ref[...]
    place = tok_slots(ids)
    tokens_in = min_ref[...]
    tokens_gr = cot_ref[...]

    def build(i, carry):
        base = (i * 64).astype(F32)
        slot = base + lax.broadcasted_iota(jnp.int32, (64, 128), 0).astype(F32)
        hits = [slot == jnp.broadcast_to(place[k], (64, 128)) for k in (0, 1)]
        pick = (hits[0] | hits[1]).astype(F32)
        weight = jnp.sum(
            jnp.where(hits[0], jnp.broadcast_to(wts[0:1, :], (64, 128)), 0.0)
            + jnp.where(hits[1], jnp.broadcast_to(wts[1:2, :], (64, 128)), 0.0),
            axis=1, keepdims=True,
        )
        pick = pick.astype(BF16)
        part_in = mm(pick, tokens_in).reshape(8, 8, 512)
        part_gr = (mm(pick, tokens_gr) * weight).reshape(8, 8, 512)
        sendbuf[pl.ds(i * 8, 8)] = jnp.concatenate([part_in, part_gr], axis=1).astype(BF16)
        return carry

    lax.fori_loop(0, 8, build, 0)
    ybuf[x, sp] = sendbuf[sp]

    pl.semaphore_wait(barrier, PEERS - 1 + 2)

    def dispatch(i, carry):
        zz = plane_at(z, lax.div(i, 8))
        m = lax.rem(me_yc + lax.rem(i, 8), 8)

        @pl.when(i != 0)
        def _():
            pltpu.make_async_remote_copy(
                src_ref=sendbuf.at[zz * 8 + m], dst_ref=ybuf.at[x, sp],
                send_sem=disp_ss.at[zz], recv_sem=disp_rs.at[z],
                device_id=peer(zz, m), device_id_type=MESH,
            ).start()

        return carry

    lax.fori_loop(0, PEERS, dispatch, 0)

    def plane_copy(buf, count, zz, ssem, rsem):
        return pltpu.make_async_remote_copy(
            src_ref=buf.at[pl.ds(zz * 8, count)], dst_ref=buf.at[pl.ds(zz * 8, count)],
            send_sem=ssem.at[zz], recv_sem=rsem.at[zz],
            device_id={"tp": right}, device_id_type=MESH,
        )

    def to_side(d, src, dst, ssem, rsem, k):
        return pltpu.make_async_remote_copy(
            src_ref=src, dst_ref=dst, send_sem=ssem.at[d, k], recv_sem=rsem.at[d, k],
            device_id={"tp": right if d == 0 else left}, device_id_type=MESH,
        )

    def a1(d, zz):
        blk = ybuf.at[x, pl.ds(zz * 8, 8)]
        return to_side(d, blk, blk, a1_s, a1_r, zz)

    def a2(d, zz):
        blk = ybuf.at[left if d == 0 else right, pl.ds(zz * 8 + 4 * d, 4)]
        return to_side(d, blk, blk, a2_s, a2_r, zz)

    def r1(d, zz):
        return to_side(d, rs1_s.at[d, zz], rs1_r.at[d, zz], r1_s, r1_r, zz)

    def r2(d, zz):
        return to_side(d, rs2_s.at[d, zz], rs2_r.at[d, zz], r2_s, r2_r, zz)


    def group_send(buf, land, m, ssem, rsem):
        return pltpu.make_async_remote_copy(
            src_ref=buf.at[m], dst_ref=land.at[me_yc], send_sem=ssem, recv_sem=rsem,
            device_id=peer(z, m), device_id_type=MESH,
        )

    def plane_send(src, land, zz, ssem, rsem):
        return pltpu.make_async_remote_copy(
            src_ref=src, dst_ref=land.at[z], send_sem=ssem, recv_sem=rsem,
            device_id=peer(zz, me_yc), device_id_type=MESH,
        )

    def seven(buf, ssem, rsem):
        blk = buf.at[pl.ds(0, 7)]
        return pltpu.make_async_remote_copy(
            src_ref=blk, dst_ref=blk, send_sem=ssem, recv_sem=rsem,
            device_id={"tp": right}, device_id_type=MESH,
        )

    def scan_a(k, state, dec):
        full = jnp.concatenate([state, two_rows(dec)], axis=0).astype(BF16)
        for j in range(8):
            msg_a[k, j] = full[:, j * 128 : (j + 1) * 128]
        rec_a[k, me_yc] = msg_a[k, me_yc]

        def go(t, carry):
            m = lax.rem(me_yc + t, 8)
            group_send(msg_a.at[k], rec_a.at[k], m, sa_s.at[k], sa_r.at[k]).start()
            return carry

        lax.fori_loop(1, 8, go, 0)

    def scan_b(k, order):
        seven(rec_a.at[k], sa_s.at[k], sa_r.at[k]).wait_recv()
        state = jnp.zeros((64, 128), F32)
        dec = jnp.ones((1, 128), F32)
        for m in order:
            pref[k, m] = state
            prefd[k, m] = jnp.broadcast_to(dec, (8, 128))
            tail = rec_a[k, m, 64:80].astype(F32)
            own = tail[0:1] + tail[1:2]
            state = state * own + rec_a[k, m, 0:64].astype(F32)
            dec = dec * own
        msg_b[k] = jnp.concatenate([state, two_rows(dec)], axis=0).astype(BF16)
        rec_b[k, z] = msg_b[k]

        def go(t, carry):
            zz = lax.rem(z + t, NZ)
            plane_send(msg_b.at[k], rec_b.at[k], zz, sb_s.at[k], sb_r.at[k]).start()
            return carry

        lax.fori_loop(1, NZ, go, 0)

    def scan_c(k, order):
        seven(rec_b.at[k], sb_s.at[k], sb_r.at[k]).wait_recv()
        state = jnp.zeros((64, 128), F32)
        for zz in order:
            tail = rec_b[k, zz, 64:80].astype(F32)
            nxt = state * (tail[0:1] + tail[1:2]) + rec_b[k, zz, 0:64].astype(F32)
            passed = (zz < z) if order[0] == 0 else (zz > z)
            state = jnp.where(passed, nxt, state)
        for m in range(8):
            msg_c[k, m] = (state * prefd[k, m][0:1] + pref[k, m]).astype(BF16)
        rec_c[k, me_yc] = msg_c[k, me_yc]

        def go(t, carry):
            m = lax.rem(me_yc + t, 8)
            group_send(msg_c.at[k], rec_c.at[k], m, sc_s.at[k], sc_r.at[k]).start()
            return carry

        lax.fori_loop(1, 8, go, 0)

    def scan_d(k):
        seven(rec_c.at[k], sc_s.at[k], sc_r.at[k]).wait_recv()
        return jnp.concatenate([rec_c[k, j] for j in range(8)], axis=1)

    up_order = tuple(range(8))
    down_order = tuple(reversed(range(8)))

    def mix_prepare():
        e = head_map()
        raw = raw_ref[...]
        step_size = jnp.maximum(raw, 0.0) + jnp.log1p(jnp.exp(-jnp.abs(raw)))
        dlog = -step_size * decay_ref[...]
        tri = (iota((128, 128), 0) >= iota((128, 128), 1)).astype(F32).astype(BF16)
        running = tri_sum(tri, dlog)
        r_ref[...] = running
        padded = jnp.concatenate([running, jnp.zeros((128, 112), F32)], axis=1)
        rt_ref[...] = padded.T
        stepx = spread(step_size, e)
        stepx_ref[...] = stepx
        erx_ref[...] = spread(jnp.exp(running), e)
        tex = spread(jnp.exp(running[127:128] - running), e)
        tex_ref[...] = tex
        xin = ix_ref[...].astype(F32)
        scaled = xin * sigmoid(xin) * stepx
        scaled_ref[...] = scaled
        bin_ = ib_ref[...].astype(F32)
        cin = ic_ref[...].astype(F32)
        b_act = (bin_ * sigmoid(bin_)).astype(BF16)
        c_act = (cin * sigmoid(cin)).astype(BF16)
        scores_ref[...] = mm(c_act, b_act, DIMS_NT)
        fresh = mm(b_act, (scaled * tex).astype(BF16), DIMS_TN)
        scan_a(0, fresh, erx_ref[127:128, :])

    def pair_forward(p, carry):
        lanes = pl.ds(pl.multiple_of(p * 128, 128), 128)
        sc = scaled_ref[:, lanes]
        low = iota((128, 128), 1) < 64
        causal = iota((128, 128), 0) >= iota((128, 128), 1)
        rhs = jnp.concatenate(
            [jnp.where(low, sc, 0.0).astype(BF16), jnp.where(low, 0.0, sc).astype(BF16)], axis=0
        )
        running = r_ref[...]
        scores = scores_ref[...]
        ms = []
        for k in (0, 1):
            h = 2 * p + k
            col = jnp.sum(jnp.where(iota((128, 16), 1) == h, running, 0.0), axis=1, keepdims=True)
            row = rt_ref[pl.ds(h, 1), :]
            w = jnp.exp(jnp.where(causal, col - row, -1e30))
            w_ref[h] = w
            ms.append((scores * w).astype(BF16))
            m_ref[h] = ms[k]
        inside_ref[:, lanes] = mm(jnp.concatenate(ms, axis=1), rhs)
        return carry

    def skip_lanes():
        return spread(jnp.broadcast_to(skip_ref[...], (8, 16)), head_map())[0:1]

    def mix_norm():
        state = scan_d(0)
        carry_ref[...] = state
        cin = ic_ref[...].astype(F32)
        c_act = (cin * sigmoid(cin)).astype(BF16)
        carried = mm(c_act, state) * erx_ref[...]
        carried_ref[...] = carried
        xin = ix_ref[...].astype(F32)
        zin = gz_ref[...].astype(F32)
        mixed = inside_ref[...] + carried + xin * sigmoid(xin) * skip_lanes()
        gated = mixed * (zin * sigmoid(zin))
        inv = lax.rsqrt(jnp.mean(gated * gated, axis=1, keepdims=True) + EPS)
        gated_ref[...] = gated
        inv_ref[...] = jnp.broadcast_to(inv, (128, 128))
        nr[me_yc] = (gated * inv * gain_ref[...]).astype(BF16)

    def n1(t):
        dev = {"sp_2": 1 - c} if t == 0 else {"sp_1": lax.rem(y + t, NY)}
        blk = nr.at[me_yc]
        return pltpu.make_async_remote_copy(
            src_ref=blk, dst_ref=blk, send_sem=n_s.at[t], recv_sem=n_r.at[t],
            device_id=dev, device_id_type=MESH,
        )

    def n2(t):
        blk = nr.at[lax.rem(y + NY - t, NY) * 2 + c]
        return pltpu.make_async_remote_copy(
            src_ref=blk, dst_ref=blk, send_sem=n_s.at[3 + t], recv_sem=n_r.at[3 + t],
            device_id={"sp_2": 1 - c}, device_id_type=MESH,
        )

    def step(i, carry):
        @pl.when(i < 8)
        def _():
            zz = plane_at(z, i)

            @pl.when(i == 0)
            def _():
                plane_copy(ybuf.at[x], 7, z, disp_ss, disp_rs).wait_recv()

            @pl.when(i > 0)
            def _():
                plane_copy(ybuf.at[x], 8, zz, disp_ss, disp_rs).wait_recv()

            a1(0, zz).start()
            a1(1, zz).start()

        @pl.when((i >= 1) & (i < 9))
        def _():
            zz = plane_at(z, i - 1)
            a1(0, zz).wait_recv()
            a2(0, zz).start()
            a1(1, zz).wait_recv()
            a2(1, zz).start()

        @pl.when((i >= 2) & (i < 10))
        def _():
            zz = plane_at(z, i - 2)
            a2(0, zz).wait_recv()
            a2(1, zz).wait_recv()

            @pl.when(i == 2)
            def _():
                for load in loads[:3]:
                    load.wait()

            gate = jnp.zeros((128, 256), F32)
            up = jnp.zeros((128, 256), F32)
            hgrad = jnp.zeros((128, 256), F32)
            for q in range(NX):
                rowsq = ybuf[q, pl.ds(zz * 8, 8)].reshape(128, 512)
                gate += mm(rowsq, gw[q])
                up += mm(rowsq, uw[q])
                hgrad += mm(rowsq, dw[:, q * 512 : (q + 1) * 512], DIMS_NT)
            gate = gate.reshape(8, 16, 256)[:, :8]
            up = up.reshape(8, 16, 256)[:, :8]
            hgrad = hgrad.reshape(8, 16, 256)[:, 8:]
            sig = 1.0 / (1.0 + jnp.exp(-gate))
            act = gate * sig
            zero = jnp.zeros((8, 8, 256), F32)
            hid[pl.ds(zz * 8, 8)] = jnp.concatenate([zero, act * up], axis=1).astype(BF16)
            gg = hgrad * up * sig * (1.0 + gate * (1.0 - sig))
            ug = hgrad * act
            ggi[pl.ds(zz * 8, 8), :, 0:256] = jnp.concatenate([gg, zero], axis=1).astype(BF16)
            ggi[pl.ds(zz * 8, 8), :, 256:512] = jnp.concatenate([ug, zero], axis=1).astype(BF16)
            ggc = gg.reshape(64, 256).astype(BF16)
            ugc = ug.reshape(64, 256).astype(BF16)

            def terms(q):
                return mm(ggc, gw[q], DIMS_NT) + mm(ugc, uw[q], DIMS_NT)

            away = terms(far).astype(BF16)
            rs1_s[0, zz] = away[:32]
            rs1_s[1, zz] = away[32:]
            r1(0, zz).start()
            r1(1, zz).start()
            nbr_acc[0, zz] = terms(right)
            nbr_acc[1, zz] = terms(left)
            own_acc[zz] = terms(x)

        @pl.when((i >= 3) & (i < 11))
        def _():
            zz = plane_at(z, i - 3)
            r1(0, zz).wait_recv()
            rs2_s[0, zz, 0:32] = (nbr_acc[0, zz, 0:32] + rs1_r[0, zz].astype(F32)).astype(BF16)
            rs2_s[0, zz, 32:64] = nbr_acc[0, zz, 32:64].astype(BF16)
            r2(0, zz).start()
            r1(1, zz).wait_recv()
            rs2_s[1, zz, 0:32] = nbr_acc[1, zz, 0:32].astype(BF16)
            rs2_s[1, zz, 32:64] = (nbr_acc[1, zz, 32:64] + rs1_r[1, zz].astype(F32)).astype(BF16)
            r2(1, zz).start()

        @pl.when(i >= 4)
        def _():
            zz = plane_at(z, i - 4)
            r2(0, zz).wait_recv()
            r2(1, zz).wait_recv()
            total = own_acc[zz] + rs2_r[0, zz].astype(F32) + rs2_r[1, zz].astype(F32)
            total = total.reshape(8, 8, 512)
            retbuf[pl.ds(zz * 8, 8)] = jnp.concatenate(
                [total[:, :, :256], total[:, :, 256:]], axis=1
            ).astype(BF16)

            @pl.when(i == 4)
            def _():
                backbuf[sp] = retbuf[sp]

            def give(k, inner):
                m = lax.rem(me_yc + k, 8)

                @pl.when((k > 0) | (i > 4))
                def _():
                    pltpu.make_async_remote_copy(
                        src_ref=retbuf.at[zz * 8 + m], dst_ref=backbuf.at[sp],
                        send_sem=ret_ss.at[zz], recv_sem=ret_rs.at[z],
                        device_id=peer(zz, m), device_id_type=MESH,
                    ).start()

                return inner

            lax.fori_loop(0, 8, give, 0)

        @pl.when(i == 0)
        def _():
            mix_prepare()

        @pl.when(i == 2)
        def _():
            scan_b(0, up_order)

        @pl.when((i >= 3) & (i < 7))
        def _():
            pair_forward(2 * (i - 3), 0)
            pair_forward(2 * (i - 3) + 1, 0)

        @pl.when(i == 4)
        def _():
            scan_c(0, up_order)

        @pl.when(i == 7)
        def _():
            mix_norm()
            for t in range(4):
                n1(t).start()

        @pl.when(i == 10)
        def _():
            for t in range(1, 4):
                n1(t).wait_recv()
                n2(t).start()

        return carry

    lax.fori_loop(0, 12, step, 0)

    def weights_in(q):
        g = mm(ybuf[q].reshape(1024, 512), ggi[...].reshape(1024, 512), DIMS_TN)
        gout[0, q] = g[:, :256].astype(BF16)
        gout[1, q] = g[:, 256:].astype(BF16)

    def weights_down(q):
        d = mm(hid[...].reshape(1024, 256), ybuf[q].reshape(1024, 512), DIMS_TN)
        dout[:, q * 512 : (q + 1) * 512] = d.astype(BF16)

    weights_in(0)
    weights_in(1)

    def arrive(k, carry):
        zz = plane_at(z, k)

        @pl.when(k == 0)
        def _():
            plane_copy(backbuf, 7, z, ret_ss, ret_rs).wait_recv()

        @pl.when(k > 0)
        def _():
            plane_copy(backbuf, 8, zz, ret_ss, ret_rs).wait_recv()

        return carry

    lax.fori_loop(0, NZ, arrive, 0)
    r_iota = lax.broadcasted_iota(jnp.int32, (128, 1024), 1)
    slot_of = ((r_iota // 16) * 8 + r_iota % 8).astype(F32)
    upper = (r_iota % 16) >= 8
    hit = (slot_of == to_column(place[0])) | (slot_of == to_column(place[1]))
    low = (hit & jnp.logical_not(upper)).astype(F32).astype(BF16)
    high = (hit & upper).astype(F32).astype(BF16)
    back = backbuf[...].reshape(1024, 256)
    moe_grad = jnp.concatenate([mm(low, back), mm(high, back)], axis=1)
    rows[x] = (tokens_gr.astype(F32) + moe_grad).astype(BF16)

    def m1(d):
        return to_side(d, rows.at[x], rows.at[x], m_s, m_r, 0)

    def m2(d):
        blk = rows.at[left if d == 0 else right, pl.ds(64 * d, 64)]
        return to_side(d, blk, blk, m_s, m_r, 1)

    m1(0).start()
    m1(1).start()
    weights_in(2)
    m1(0).wait_recv()
    m2(0).start()
    m1(1).wait_recv()
    m2(1).start()
    weights_in(3)
    m2(0).wait_recv()
    m2(1).wait_recv()

    for q in range(NX):
        turned[2 * q : 2 * q + 2] = rows[q].T.reshape(2, 8, 32, 128)
    turned_in[me_yc] = turned[:, me_yc]

    def t1(m):
        return pltpu.make_async_remote_copy(
            src_ref=turned.at[:, m], dst_ref=turned_in.at[me_yc],
            send_sem=t1_s.at[0], recv_sem=t1_r.at[0],
            device_id=peer(z, m), device_id_type=MESH,
        )

    def t1_go(t, carry):
        t1(lax.rem(me_yc + t, 8)).start()
        return carry

    lax.fori_loop(1, 8, t1_go, 0)

    loads[3].wait()
    norm_grad = mm(rows[0], wo[0])
    for q in range(1, NX):
        norm_grad += mm(rows[q], wo[q])
    inv = inv_ref[:, 0:1]
    gated = gated_ref[...]
    scale = norm_grad * gain_ref[...]
    dgated = scale * inv - gated * (inv * inv * inv * jnp.mean(gated * scale, axis=1, keepdims=True))
    zin = gz_ref[...].astype(F32)
    zsig = sigmoid(zin)
    dmix = dgated * (zin * zsig)
    dy_ref[...] = dmix
    cin = ic_ref[...].astype(F32)
    c_sig = sigmoid(cin)
    c_act = (cin * c_sig).astype(BF16)
    leaving = (dmix * erx_ref[...]).astype(BF16)
    scan_a(1, mm(c_act, leaving, DIMS_TN), erx_ref[127:128, :])
    xin = ix_ref[...].astype(F32)
    xsig = sigmoid(xin)
    mixed = inside_ref[...] + carried_ref[...] + xin * xsig * skip_lanes()
    gzz_ref[...] = (dgated * mixed * (zsig * (1.0 + zin * (1.0 - zsig)))).astype(BF16)
    dsc_ref[...] = jnp.zeros((128, 128), F32)

    def pair_back(p, carry):
        lanes = pl.ds(pl.multiple_of(p * 128, 128), 128)
        dy = dy_ref[:, lanes]
        low = iota((128, 128), 1) < 64
        both = jnp.concatenate(
            [jnp.where(low, dy, 0.0).astype(BF16), jnp.where(low, 0.0, dy).astype(BF16)], axis=0
        )
        ds1_ref[:, lanes] = mm(m_ref[pl.ds(2 * p, 2)].reshape(256, 128), both, DIMS_TN)
        dm = mm(both, scaled_ref[:, lanes].astype(BF16), DIMS_NT)
        dsc_ref[...] += dm[:128] * w_ref[2 * p] + dm[128:] * w_ref[2 * p + 1]
        return carry

    lax.fori_loop(0, 4, pair_back, 0)
    scan_b(1, down_order)
    n1(0).wait_recv()
    for t in range(1, 4):
        n2(t).wait_recv()
    seven(turned_in, t1_s.at[0], t1_r.at[0]).wait_recv()
    terms_out = mm(turned_in[0].reshape(256, 128), nr[0])
    for m in range(1, 8):
        terms_out += mm(turned_in[m].reshape(256, 128), nr[m])
    part[...] = terms_out.reshape(8, 32, 1024).astype(BF16)
    parts_in[z] = part[z]

    def t2_go(t, carry):
        zz = lax.rem(z + t, NZ)
        plane_send(part.at[zz], parts_in, zz, t2_s.at[0], t2_r.at[0]).start()
        return carry

    lax.fori_loop(1, NZ, t2_go, 0)
    lax.fori_loop(4, 8, pair_back, 0)
    scan_c(1, down_order)
    state = carry_ref[...]
    dsc = dsc_ref[...].astype(BF16)
    bin_ = ib_ref[...].astype(F32)
    b_sig = sigmoid(bin_)
    b_act = (bin_ * b_sig).astype(BF16)
    dc = mm(dsc, b_act) + mm(leaving, state, DIMS_NT)
    gc_ref[...] = dc * (c_sig * (1.0 + cin * (1.0 - c_sig)))
    e = head_map()
    dmix_b = dmix.astype(BF16).astype(F32)
    scaled = scaled_ref[...]
    scaled_b = scaled.astype(BF16).astype(F32)
    ds1 = ds1_ref[...]
    turn = per_head(dmix_b * inside_ref[...] + dmix * carried_ref[...] - scaled_b * ds1, e)
    for q in range(2):
        weights_down(q)
    after = scan_d(1)
    tex = tex_ref[...]
    ds2 = mm(b_act, after) * tex
    db = mm(dsc, c_act, DIMS_TN) + mm((scaled * tex).astype(BF16), after, DIMS_NT)
    gb_ref[...] = db * (b_sig * (1.0 + bin_ * (1.0 - b_sig)))
    dscaled = ds1 + ds2
    gx_ref[...] = (
        (dscaled * stepx_ref[...] + dmix * skip_lanes()) * (xsig * (1.0 + xin * (1.0 - xsig)))
    ).astype(BF16)
    fade = per_head(scaled * ds2, e)
    at_end = jnp.sum(after.astype(F32) * state.astype(F32), axis=0, keepdims=True)
    at_end = per_head(jnp.broadcast_to(at_end, (8, 1024)), e)[0:1]
    at_end = jnp.sum(fade, axis=0, keepdims=True) + at_end * jnp.exp(r_ref[127:128, :])
    later = (iota((128, 128), 0) <= iota((128, 128), 1)).astype(F32).astype(BF16)
    dlog_grad = tri_sum(later, turn - fade) + at_end
    raw = raw_ref[...]
    dstep = per_head(dscaled * (xin * xsig), e) - dlog_grad * decay_ref[...]
    graw_ref[...] = dstep * sigmoid(raw)
    for q in range(2, NX):
        weights_down(q)
    outs = [
        pltpu.make_async_copy(src, dst, o_sem.at[k])
        for k, (src, dst) in enumerate(((gout.at[0], gwg_hbm), (gout.at[1], uwg_hbm), (dout, dwg_hbm)))
    ]
    for out in outs:
        out.start()
    seven(parts_in, t2_s.at[0], t2_r.at[0]).wait_recv()
    total = parts_in[0].astype(F32)
    for zz in range(1, NZ):
        total += parts_in[zz].astype(F32)
    go_ref[...] = total

    def drain(k, carry):
        @pl.when(k == z)
        def _():
            plane_copy(sendbuf, 7, k, disp_ss, disp_rs).wait_send()
            plane_copy(retbuf, 7, k, ret_ss, ret_rs).wait_send()

        @pl.when(k != z)
        def _():
            plane_copy(sendbuf, 8, k, disp_ss, disp_rs).wait_send()
            plane_copy(retbuf, 8, k, ret_ss, ret_rs).wait_send()

        for d in (0, 1):
            a1(d, k).wait_send()
            a2(d, k).wait_send()
            r1(d, k).wait_send()
            r2(d, k).wait_send()
        return carry

    lax.fori_loop(0, NZ, drain, 0)
    for d in (0, 1):
        m1(d).wait_send()
        m2(d).wait_send()
    for k in (0, 1):
        seven(msg_a.at[k], sa_s.at[k], sa_r.at[k]).wait_send()
        seven(rec_b.at[k], sb_s.at[k], sb_r.at[k]).wait_send()
        seven(msg_c.at[k], sc_s.at[k], sc_r.at[k]).wait_send()
    for t in range(4):
        n1(t).wait_send()
    for t in range(1, 4):
        n2(t).wait_send()
    seven(turned_in, t1_s.at[0], t1_r.at[0]).wait_send()
    seven(part, t2_s.at[0], t2_r.at[0]).wait_send()
    for out in outs:
        out.wait()


def fused_call(
    moe_input, cotangent, expert_ids, routing_weights, gate_weight, up_weight, down_weight,
    inner_x, inner_b, inner_c, gate_z, step_raw, decay_rate, skip_weight, norm_gain, w_out,
):
    vmem = pl.BlockSpec(memory_space=pltpu.VMEM)
    hbm = pl.BlockSpec(memory_space=pl.ANY)
    dma = pltpu.SemaphoreType.DMA
    V = pltpu.VMEM
    S = jax.ShapeDtypeStruct
    sems = [dma((4,)), dma((3,)), dma((8,)), dma((8,)), dma((8,)), dma((8,))]
    sems += [dma((2, 8))] * 8 + [dma((2, 2))] * 2
    wide = V((128, 1024), F32)
    go, gx, gb, gc, gzz, graw, gwg, uwg, dwg = pl.pallas_call(
        fused_kernel,
        name="fused",
        out_shape=(
            S((32, 1024), F32), S((128, 1024), BF16), S((128, 64), F32), S((128, 64), F32),
            S((128, 1024), BF16), S((128, 16), F32),
            S((NX, 512, 256), BF16), S((NX, 512, 256), BF16), S((256, 2048), BF16),
        ),
        in_specs=[vmem] * 12 + [hbm] * 4,
        out_specs=(vmem,) * 6 + (hbm,) * 3,
        scratch_shapes=[
            V((64, 16, 512), BF16), V((NX, 64, 16, 512), BF16),
            V((NX, 512, 256), BF16), V((NX, 512, 256), BF16), V((256, 2048), BF16),
            V((8, 64, 512), F32), V((2, 8, 64, 512), F32),
            V((2, 8, 32, 512), BF16), V((2, 8, 32, 512), BF16),
            V((2, 8, 64, 512), BF16), V((2, 8, 64, 512), BF16),
            V((64, 16, 512), BF16), V((64, 16, 256), BF16),
            V((64, 16, 256), BF16), V((64, 16, 256), BF16),
            V((NX, 128, 512), BF16), V((2, NX, 512, 256), BF16), V((256, 2048), BF16),
        ] + sems + [
            V((NX, 512, 1024), BF16), wide, wide, wide, wide, V((128, 16), F32),
            V((128, 128), F32), V((128, 128), F32), V((16, 128, 128), F32),
            V((16, 128, 128), BF16), wide, V((64, 1024), BF16), wide,
            V((8, 128, 1024), BF16), wide, V((128, 128), F32), wide, wide, V((128, 128), F32),
            V((2, 8, 80, 128), BF16), V((2, 8, 80, 128), BF16), V((2, 80, 128), BF16),
            V((2, 8, 80, 128), BF16), V((2, 8, 64, 128), BF16), V((2, 8, 64, 128), BF16),
            V((2, 8, 64, 128), F32), V((2, 8, 8, 128), F32),
            V((8, 8, 32, 128), BF16), V((8, 8, 32, 128), BF16),
            V((8, 32, 1024), BF16), V((8, 32, 1024), BF16),
        ] + [dma((2,))] * 6 + [dma((7,))] * 2 + [dma((1,))] * 4,
        compiler_params=pltpu.CompilerParams(
            collective_id=0, has_side_effects=True, vmem_limit_bytes=63 * 1024 * 1024
        ),
    )(
        expert_ids.T, routing_weights.T, moe_input, cotangent,
        inner_x, inner_b, inner_c, gate_z, step_raw,
        decay_rate.reshape(1, 16), skip_weight.reshape(1, 16), norm_gain.reshape(1, 1024),
        gate_weight.reshape(NX, 512, 256), up_weight.reshape(NX, 512, 256),
        down_weight.reshape(256, 2048), w_out.reshape(NX, 512, 1024),
    )
    return (
        gwg.reshape(1, 2048, 256), uwg.reshape(1, 2048, 256), dwg.reshape(1, 256, 2048),
        go, gx, gb, gc, gzz, graw,
    )


def solution(mesh):
    finer = Mesh(mesh.devices.reshape(8, 4, 2, mesh.shape["tp"]), ("sp_0", "sp_1", "sp_2", "tp"))
    return jax.shard_map(
        fused_call,
        mesh=finer,
        in_specs=(
            P(SP, "tp"),
            P(SP, "tp"),
            P(SP, None),
            P(SP, None),
            P(SP, None, "tp"),
            P(SP, None, "tp"),
            P(SP, "tp", None),
            P(SP, "tp"),
            P(SP, "tp"),
            P(SP, "tp"),
            P(SP, "tp"),
            P(SP, "tp"),
            P("tp"),
            P("tp"),
            P("tp"),
            P(None, "tp"),
        ),
        out_specs=(
            P(SP, None, "tp"),
            P(SP, None, "tp"),
            P(SP, "tp", None),
            P(SP, "tp"),
            P(SP, "tp"),
            P(SP, "tp"),
            P(SP, "tp"),
            P(SP, "tp"),
            P(SP, "tp"),
        ),
        check_vma=False,
    )
```

time: 421 us -> 139 us (0.33)
  waiting for transfers between devices: 142 us -> 0 us
  blocking collectives: 126 us -> 0 us
  Pallas kernels: 0 us -> 121 us
  matrix products: 42.9 us -> 0 us
  other arithmetic: 33.8 us -> 0 us
  local copies, waits for them, and re-layouts: 37.4 us -> 16.6 us
  starting transfers between devices: 20.2 us -> 0 us
  between operations: 17.4 us -> 0.69 us
    pallas_call x0 -> x1, Pallas kernels: none -> 121 us  [fused_call(): pl.pallas_call(fused_kernel, name='fused', out_shape=(S((32, 1024), F32),...]
    reduce_scatter x3 -> x0, waiting for transfers between devices: 103 us -> none  [own_rows(): subtotal = lax.psum_scatter(subtotal, axis, scatter_dimension=0, tiled=True)]
    all_gather x7 -> x0, blocking collectives: 81.7 us -> none  [the longest x4 51.1 us: prefix_by_axis(): lax.all_gather(part.astype(kind), axis)]
    dot_general x24 -> x0, matrix products: 42.9 us -> none  [the longest x3 7.11 us: block_outputs(): jnp.einsum('lgn,gepn,lge->lgep', c_block, carry_state, jnp.exp(running))]
    all_to_all x1 -> x0, blocking collectives: 41.1 us -> none  [sent_together(): lax.all_to_all(both, axis, split_axis=split_dim, concat_axis=concat_dim,...]
    all_gather x3 -> x0, waiting for transfers between devices: 28.8 us -> none  [the longest x1 28.8 us: in_one_piece(): lax.all_gather(both, axis, axis=dim, tiled=True)]
    all_to_all x3 -> x0, starting transfers between devices: 19.6 us -> none  [the longest x1 11.7 us: body(): lax.all_to_all(summed, SP, split_axis=0, concat_axis=0, tiled=True)]
    unnamed x198 -> x20, local copies, waits for them, and re-layouts: 6.01 us -> 16.6 us
  transfers between devices with their start and end apart: 9 -> 0, of which waited for: 6 -> 0; matrix products, arithmetic and copies ran while one was open for 19% -> 0% of each run, Pallas kernels for 0% -> 0%
where the time goes in v1:
time: 139 us; the launch traced here: 138 us
  Pallas kernels  121 us (87%)
  local copies, waits for them, and re-layouts  16.6 us (12%)
    pallas_call x1, Pallas kernels, fused_call(): pl.pallas_call(fused_kernel, name='fused', out_shape=(S((32, 1024), F32),...  121 us
    unnamed x20, local copies, waits for them, and re-layouts  16.6 us

profile of v1, /device:TPU:1, one launch (start us, length us, event | category | flops | bytes accessed | tf_op | source)
XLA Modules:
  0.0 138.2 jit_solution(5936131913169877090)
XLA Ops:
  0.6 1.4 %copy.25.ib_ref = bf16[128,64]{1,0:T(8,128)(2,1)} copy(bf16[128,64]{0,1:T(8,128)(2,1)} %param.24) | data formatting | bytes 32768 | tf_op args[8]
  2.1 1.4 %copy.26.ic_ref = bf16[128,64]{1,0:T(8,128)(2,1)} copy(bf16[128,64]{0,1:T(8,128)(2,1)} %param.25) | data formatting | bytes 32768 | tf_op args[9]
  3.5 1.4 %copy.27.raw_ref = f32[128,16]{1,0:T(8,128)} copy(f32[128,16]{0,1:T(8,128)} %param.27) | data formatting | bytes 16384 | tf_op args[11]
  4.9 120.9 %fused.1 = (f32[32,1024]{1,0:T(8,128)}, bf16[128,1024]{1,0:T(8,128)(2,1)}, f32[128,64]{1,0:T(8,128)}, f32[128,64]{1,0:T(8,128)}, bf16[128,1024]{1,0:T(8,128)(2,1...) custom-call(s32[2,128]{1,0:T(2,128)} %bitcast.20, ...), custom_call_target="tpu_custom_call" | custom-call | tf_op jit(solution)/shard_map/fused/pallas_call | solution.py:736
  125.9 0.0 copy-start
  125.9 0.0 copy-start.3
  125.9 0.0 copy-start.2
  125.9 0.0 copy-start.1
  125.9 1.6 %copy.30 = f32[128,16]{0,1:T(8,128)} copy(f32[128,16]{1,0:T(8,128)} %get-tuple-element.35) | data formatting | bytes 16384
  127.5 1.5 %copy.28 = f32[128,64]{0,1:T(8,128)} copy(f32[128,64]{1,0:T(8,128)} %get-tuple-element.32) | data formatting | bytes 65536
  129.1 1.5 %copy.29 = f32[128,64]{0,1:T(8,128)} copy(f32[128,64]{1,0:T(8,128)} %get-tuple-element.33) | data formatting | bytes 65536
  130.6 2.3 %copy.37 = bf16[1,2048,256]{2,1,0:T(8,128)(2,1)} copy(bf16[1,2048,256]{2,1,0:T(8,128)(2,1)} %bitcast.18) | data formatting | bytes 2097152
  132.9 2.3 %copy.38 = bf16[1,2048,256]{2,1,0:T(8,128)(2,1)} copy(bf16[1,2048,256]{2,1,0:T(8,128)(2,1)} %bitcast.17) | data formatting | bytes 2097152
  135.1 0.0 copy-done
  135.1 1.0 copy.39
  136.1 0.0 copy-done.3
  136.1 0.7 copy.40
  136.8 0.0 copy-done.2
  136.8 0.7 copy.41
  137.5 0.0 copy-done.1
  137.5 0.7 copy.42
Async XLA Ops:
  125.9 9.3 %copy-start = (bf16[256,2048]{1,0:T(8,128)(2,1)S(1)}, bf16[256,2048]{1,0:T(8,128)(2,1)}, u32[]{:S(2)}) copy-start(bf16[256,2048]{1,0:T(8,128)(2,1)} %get-tuple-element.20) | copy-start | bytes 3145732
  125.9 10.2 %copy-start.3 = (f32[32,1024]{1,0:T(8,128)S(1)}, f32[32,1024]{1,0:T(8,128)}, u32[]{:S(2)}) copy-start(f32[32,1024]{1,0:T(8,128)} %get-tuple-element.48) | copy-start | bytes 393220
  125.9 10.9 %copy-start.2 = (bf16[128,1024]{1,0:T(8,128)(2,1)S(1)}, bf16[128,1024]{1,0:T(8,128)(2,1)}, u32[]{:S(2)}) copy-start(bf16[128,1024]{1,0:T(8,128)(2,1)} %get-tuple-element.49) | copy-start | bytes 786436
  125.9 11.6 %copy-start.1 = (bf16[128,1024]{1,0:T(8,128)(2,1)S(1)}, bf16[128,1024]{1,0:T(8,128)(2,1)}, u32[]{:S(2)}) copy-start(bf16[128,1024]{1,0:T(8,128)(2,1)} %get-tuple-element.52) | copy-start | bytes 786436

commit v2 on v1

--- a/solution.py
+++ b/solution.py
@@ -22,10 +22,15 @@
     return lax.dot_general(a, b, dims, preferred_element_type=F32)
 
 
+def offset_at(i):
+    off = jnp.int32(0)
+    for k, at in enumerate((0, 1, 7, 2, 6, 4, 3, 5)):
+        off = jnp.where(i == k, at, off)
+    return off
+
+
 def plane_at(z, i):
-    odd = lax.rem(i, 2)
-    off = odd * lax.div(i + 1, 2) + (1 - odd) * (NZ - lax.div(i, 2))
-    return lax.rem(z + off, NZ)
+    return lax.rem(z + offset_at(i), NZ)
 
 
 def tok_slots(ids):
@@ -86,6 +91,14 @@
     return (lax.div(iota((16, 1024), 1), 64) == iota((16, 1024), 0)).astype(F32).astype(BF16)
 
 
+def upright(narrow):
+    return jnp.concatenate([narrow, jnp.zeros((112, 128), F32)], axis=0).T[:, 0:16]
+
+
+def flat(narrow):
+    return jnp.concatenate([narrow, jnp.zeros((128, 112), F32)], axis=1).T[0:16]
+
+
 def two_rows(dec):
     hi = dec.astype(BF16).astype(F32)
     row = iota((16, dec.shape[1]), 0)
@@ -93,17 +106,20 @@
 
 
 def fused_kernel(
-    ids_ref, wts_ref, min_ref, cot_ref, ix_ref, ib_ref, ic_ref, gz_ref, raw_ref, decay_ref,
-    skip_ref, gain_ref, gw_hbm, uw_hbm, dw_hbm, wo_hbm,
-    go_ref, gx_ref, gb_ref, gc_ref, gzz_ref, graw_ref, gwg_hbm, uwg_hbm, dwg_hbm,
+    ids_hbm, wts_hbm, min_hbm, cot_hbm, ix_hbm, ib_hbm, ic_hbm, gz_hbm, raw_hbm, decay_hbm,
+    skip_hbm, gain_hbm, gw_hbm, uw_hbm, dw_hbm, wo_hbm,
+    go_hbm, gx_hbm, gb_hbm, gc_hbm, gzz_hbm, graw_hbm, gwg_hbm, uwg_hbm, dwg_hbm,
     sendbuf, ybuf, gw, uw, dw, own_acc, nbr_acc, rs1_s, rs1_r, rs2_s, rs2_r,
     ggi, hid, retbuf, backbuf, rows, gout, dout,
     w_sem, o_sem, disp_ss, disp_rs, ret_ss, ret_rs,
     a1_s, a1_r, a2_s, a2_r, r1_s, r1_r, r2_s, r2_r, m_s, m_r,
-    wo, scaled_ref, stepx_ref, erx_ref, tex_ref, r_ref, rt_ref, scores_ref, w_ref, m_ref,
+    go_ref, gx_ref, gb_ref, gc_ref, gzz_ref, graw_ref, bmsg_a, brec_a, bmsg_b, brec_b,
+    carried_back, far_in, bb_s, bb_r, t3_s, t3_r,
+    ids_ref, wts_ref, min_ref, cot_ref, ix_ref, ib_ref, ic_ref, gz_ref, raw_ref, decay_ref,
+    skip_ref, gain_ref, wo, scaled_ref, stepx_ref, erx_ref, tex_ref, r_ref, rt_ref, scores_ref, w_ref, m_ref,
     inside_ref, carry_ref, carried_ref, nr, gated_ref, inv_ref, dy_ref, ds1_ref, dsc_ref,
-    msg_a, rec_a, msg_b, rec_b, msg_c, rec_c, pref, prefd, turned, turned_in, part, parts_in,
-    sa_s, sa_r, sb_s, sb_r, sc_s, sc_r, n_s, n_r, t1_s, t1_r, t2_s, t2_r,
+    msg_a, rec_a, msg_b, rec_b, msg_c, rec_c, pref, prefd, turned, tin, part, parts_in,
+    sa_s, sa_r, sb_s, sb_r, sc_s, sc_r, n_s, n_r, t1_s, t1_r, t2_s, t2_r, u_s, u_r,
 ):
     z, y, c, x = (lax.axis_index(a) for a in ("sp_0", "sp_1", "sp_2", "tp"))
     sp = z * 8 + y * 2 + c
@@ -116,6 +132,18 @@
 
     barrier = pltpu.get_barrier_semaphore()
 
+    loads = [
+        pltpu.make_async_copy(src, dst, w_sem.at[k])
+        for k, (src, dst) in enumerate((
+            (ids_hbm, ids_ref), (wts_hbm, wts_ref), (min_hbm, min_ref), (cot_hbm, cot_ref),
+            (ix_hbm, ix_ref), (ib_hbm, ib_ref), (ic_hbm, ic_ref), (gz_hbm, gz_ref),
+            (raw_hbm, raw_ref), (decay_hbm, decay_ref), (skip_hbm, skip_ref), (gain_hbm, gain_ref),
+            (gw_hbm, gw), (uw_hbm, uw), (dw_hbm, dw), (wo_hbm, wo),
+        ))
+    ]
+    for load in loads[:4]:
+        load.start()
+
     def greet(i, carry):
         zz, m = lax.div(i, 8), lax.rem(i, 8)
 
@@ -129,12 +157,10 @@
     for side in (right, left):
         pl.semaphore_signal(barrier, inc=1, device_id={"tp": side}, device_id_type=MESH)
 
-    loads = [
-        pltpu.make_async_copy(src, dst, w_sem.at[k])
-        for k, (src, dst) in enumerate(((gw_hbm, gw), (uw_hbm, uw), (dw_hbm, dw), (wo_hbm, wo)))
-    ]
-    for load in loads:
+    for load in loads[4:]:
         load.start()
+    for load in loads[:4]:
+        load.wait()
 
     ids = ids_ref[...]
     wts = wts_ref[...]
@@ -164,47 +190,49 @@
     pl.semaphore_wait(barrier, PEERS - 1 + 2)
 
     def dispatch(i, carry):
-        zz = plane_at(z, lax.div(i, 8))
+        zz = lax.rem(z + NZ - offset_at(lax.div(i, 8)), NZ)
         m = lax.rem(me_yc + lax.rem(i, 8), 8)
 
         @pl.when(i != 0)
         def _():
             pltpu.make_async_remote_copy(
                 src_ref=sendbuf.at[zz * 8 + m], dst_ref=ybuf.at[x, sp],
-                send_sem=disp_ss.at[zz], recv_sem=disp_rs.at[z],
+                send_sem=disp_ss.at[0], recv_sem=disp_rs.at[z],
                 device_id=peer(zz, m), device_id_type=MESH,
             ).start()
 
         return carry
 
-    lax.fori_loop(0, PEERS, dispatch, 0)
+    lax.fori_loop(0, 8, dispatch, 0)
+
+    def waiter(blk, ssem, rsem):
+        return pltpu.make_async_remote_copy(
+            src_ref=blk, dst_ref=blk, send_sem=ssem, recv_sem=rsem,
+            device_id={"tp": right}, device_id_type=MESH,
+        )
 
     def plane_copy(buf, count, zz, ssem, rsem):
+        return waiter(buf.at[pl.ds(zz * 8, count)], ssem.at[0], rsem.at[zz])
+
+    def to_side(d, src, dst, ssem, rsem):
         return pltpu.make_async_remote_copy(
-            src_ref=buf.at[pl.ds(zz * 8, count)], dst_ref=buf.at[pl.ds(zz * 8, count)],
-            send_sem=ssem.at[zz], recv_sem=rsem.at[zz],
-            device_id={"tp": right}, device_id_type=MESH,
-        )
-
-    def to_side(d, src, dst, ssem, rsem, k):
-        return pltpu.make_async_remote_copy(
-            src_ref=src, dst_ref=dst, send_sem=ssem.at[d, k], recv_sem=rsem.at[d, k],
+            src_ref=src, dst_ref=dst, send_sem=ssem, recv_sem=rsem,
             device_id={"tp": right if d == 0 else left}, device_id_type=MESH,
         )
 
     def a1(d, zz):
         blk = ybuf.at[x, pl.ds(zz * 8, 8)]
-        return to_side(d, blk, blk, a1_s, a1_r, zz)
+        return to_side(d, blk, blk, a1_s.at[0], a1_r.at[d, zz])
 
     def a2(d, zz):
         blk = ybuf.at[left if d == 0 else right, pl.ds(zz * 8 + 4 * d, 4)]
-        return to_side(d, blk, blk, a2_s, a2_r, zz)
+        return to_side(d, blk, blk, a2_s.at[0], a2_r.at[zz])
 
     def r1(d, zz):
-        return to_side(d, rs1_s.at[d, zz], rs1_r.at[d, zz], r1_s, r1_r, zz)
+        return to_side(d, rs1_s.at[d, zz], rs1_r.at[d, zz], r1_s.at[0], r1_r.at[d, zz])
 
     def r2(d, zz):
-        return to_side(d, rs2_s.at[d, zz], rs2_r.at[d, zz], r2_s, r2_r, zz)
+        return to_side(d, rs2_s.at[d, zz], rs2_r.at[d, zz], r2_s.at[0], r2_r.at[zz])
 
 
     def group_send(buf, land, m, ssem, rsem):
@@ -226,55 +254,54 @@
             device_id={"tp": right}, device_id_type=MESH,
         )
 
-    def scan_a(k, state, dec):
+    def scan_a(state, dec):
         full = jnp.concatenate([state, two_rows(dec)], axis=0).astype(BF16)
         for j in range(8):
-            msg_a[k, j] = full[:, j * 128 : (j + 1) * 128]
-        rec_a[k, me_yc] = msg_a[k, me_yc]
+            msg_a[j] = full[:, j * 128 : (j + 1) * 128]
+        rec_a[me_yc] = msg_a[me_yc]
 
         def go(t, carry):
             m = lax.rem(me_yc + t, 8)
-            group_send(msg_a.at[k], rec_a.at[k], m, sa_s.at[k], sa_r.at[k]).start()
+            group_send(msg_a, rec_a, m, sa_s.at[0], sa_r.at[0]).start()
             return carry
 
         lax.fori_loop(1, 8, go, 0)
 
-    def scan_b(k, order):
-        seven(rec_a.at[k], sa_s.at[k], sa_r.at[k]).wait_recv()
+    def scan_b():
+        seven(rec_a, sa_s.at[0], sa_r.at[0]).wait_recv()
         state = jnp.zeros((64, 128), F32)
         dec = jnp.ones((1, 128), F32)
-        for m in order:
-            pref[k, m] = state
-            prefd[k, m] = jnp.broadcast_to(dec, (8, 128))
-            tail = rec_a[k, m, 64:80].astype(F32)
+        for m in up_order:
+            pref[m] = state
+            prefd[m] = jnp.broadcast_to(dec, (8, 128))
+            tail = rec_a[m, 64:80].astype(F32)
             own = tail[0:1] + tail[1:2]
-            state = state * own + rec_a[k, m, 0:64].astype(F32)
+            state = state * own + rec_a[m, 0:64].astype(F32)
             dec = dec * own
-        msg_b[k] = jnp.concatenate([state, two_rows(dec)], axis=0).astype(BF16)
-        rec_b[k, z] = msg_b[k]
+        msg_b[...] = jnp.concatenate([state, two_rows(dec)], axis=0).astype(BF16)
+        rec_b[z] = msg_b[...]
 
         def go(t, carry):
             zz = lax.rem(z + t, NZ)
-            plane_send(msg_b.at[k], rec_b.at[k], zz, sb_s.at[k], sb_r.at[k]).start()
+            plane_send(msg_b, rec_b, zz, sb_s.at[0], sb_r.at[0]).start()
             return carry
 
         lax.fori_loop(1, NZ, go, 0)
 
-    def scan_c(k, order):
-        seven(rec_b.at[k], sb_s.at[k], sb_r.at[k]).wait_recv()
+    def scan_c():
+        seven(rec_b, sb_s.at[0], sb_r.at[0]).wait_recv()
         state = jnp.zeros((64, 128), F32)
-        for zz in order:
-            tail = rec_b[k, zz, 64:80].astype(F32)
-            nxt = state * (tail[0:1] + tail[1:2]) + rec_b[k, zz, 0:64].astype(F32)
-            passed = (zz < z) if order[0] == 0 else (zz > z)
-            state = jnp.where(passed, nxt, state)
+        for zz in up_order:
+            tail = rec_b[zz, 64:80].astype(F32)
+            nxt = state * (tail[0:1] + tail[1:2]) + rec_b[zz, 0:64].astype(F32)
+            state = jnp.where(zz < z, nxt, state)
         for m in range(8):
-            msg_c[k, m] = (state * prefd[k, m][0:1] + pref[k, m]).astype(BF16)
-        rec_c[k, me_yc] = msg_c[k, me_yc]
+            msg_c[0, m] = (state * prefd[m][0:1] + pref[m]).astype(BF16)
+        rec_c[0, me_yc] = msg_c[0, me_yc]
 
         def go(t, carry):
             m = lax.rem(me_yc + t, 8)
-            group_send(msg_c.at[k], rec_c.at[k], m, sc_s.at[k], sc_r.at[k]).start()
+            group_send(msg_c.at[0], rec_c.at[0], m, sc_s.at[0], sc_r.at[0]).start()
             return carry
 
         lax.fori_loop(1, 8, go, 0)
@@ -286,16 +313,86 @@
     up_order = tuple(range(8))
     down_order = tuple(reversed(range(8)))
 
+    def decay_row(tail):
+        tail = tail.astype(F32)
+        return tail[0:1] + tail[1:2]
+
+    def back_a(state):
+        full = state.astype(BF16)
+        for j in range(8):
+            bmsg_a[j] = full[:, j * 128 : (j + 1) * 128]
+        brec_a[me_yc] = bmsg_a[me_yc]
+
+        def go(t, carry):
+            m = lax.rem(me_yc + t, 8)
+            group_send(bmsg_a, brec_a, m, sa_s.at[1], sa_r.at[1]).start()
+            return carry
+
+        lax.fori_loop(1, 8, go, 0)
+
+    def back_send(zz):
+        return pltpu.make_async_remote_copy(
+            src_ref=bmsg_b, dst_ref=brec_b.at[z], send_sem=bb_s.at[zz], recv_sem=bb_r.at[z],
+            device_id=peer(zz, me_yc), device_id_type=MESH,
+        )
+
+    def back_recv(zz):
+        return pltpu.make_async_remote_copy(
+            src_ref=bmsg_b, dst_ref=brec_b.at[zz], send_sem=bb_s.at[zz], recv_sem=bb_r.at[zz],
+            device_id={"tp": right}, device_id_type=MESH,
+        )
+
+    def back_b():
+        seven(brec_a, sa_s.at[1], sa_r.at[1]).wait_recv()
+        state = jnp.zeros((64, 128), F32)
+        dec = jnp.ones((1, 128), F32)
+        for m in down_order:
+            pref[m] = state
+            prefd[m] = jnp.broadcast_to(dec, (8, 128))
+            own = decay_row(rec_a[m, 64:80])
+            state = state * own + brec_a[m].astype(F32)
+            dec = dec * own
+        bmsg_b[...] = state.astype(BF16)
+        for zz in down_order:
+
+            @pl.when(zz < z)
+            def _():
+                back_send(zz).start()
+
+    def back_c():
+        carried_back[...] = jnp.zeros((64, 128), F32)
+        for zz in down_order[:-1]:
+
+            @pl.when(zz > z)
+            def _():
+                back_recv(zz).wait_recv()
+                carried_back[...] = carried_back[...] * decay_row(rec_b[zz, 64:80]) + brec_b[
+                    zz
+                ].astype(F32)
+
+        state = carried_back[...]
+        for m in range(8):
+            msg_c[1, m] = (state * prefd[m][0:1] + pref[m]).astype(BF16)
+        rec_c[1, me_yc] = msg_c[1, me_yc]
+
+        def go(t, carry):
+            m = lax.rem(me_yc + t, 8)
+            group_send(msg_c.at[1], rec_c.at[1], m, sc_s.at[1], sc_r.at[1]).start()
+            return carry
+
+        lax.fori_loop(1, 8, go, 0)
+
     def mix_prepare():
+        for load in loads[4:12]:
+            load.wait()
         e = head_map()
-        raw = raw_ref[...]
+        raw = upright(raw_ref[...])
         step_size = jnp.maximum(raw, 0.0) + jnp.log1p(jnp.exp(-jnp.abs(raw)))
         dlog = -step_size * decay_ref[...]
         tri = (iota((128, 128), 0) >= iota((128, 128), 1)).astype(F32).astype(BF16)
         running = tri_sum(tri, dlog)
         r_ref[...] = running
-        padded = jnp.concatenate([running, jnp.zeros((128, 112), F32)], axis=1)
-        rt_ref[...] = padded.T
+        rt_ref[...] = flat(running)
         stepx = spread(step_size, e)
         stepx_ref[...] = stepx
         erx_ref[...] = spread(jnp.exp(running), e)
@@ -304,13 +401,13 @@
         xin = ix_ref[...].astype(F32)
         scaled = xin * sigmoid(xin) * stepx
         scaled_ref[...] = scaled
-        bin_ = ib_ref[...].astype(F32)
-        cin = ic_ref[...].astype(F32)
+        bin_ = ib_ref[...].astype(F32).T
+        cin = ic_ref[...].astype(F32).T
         b_act = (bin_ * sigmoid(bin_)).astype(BF16)
         c_act = (cin * sigmoid(cin)).astype(BF16)
         scores_ref[...] = mm(c_act, b_act, DIMS_NT)
         fresh = mm(b_act, (scaled * tex).astype(BF16), DIMS_TN)
-        scan_a(0, fresh, erx_ref[127:128, :])
+        scan_a(fresh, erx_ref[127:128, :])
 
     def pair_forward(p, carry):
         lanes = pl.ds(pl.multiple_of(p * 128, 128), 128)
@@ -340,7 +437,7 @@
     def mix_norm():
         state = scan_d(0)
         carry_ref[...] = state
-        cin = ic_ref[...].astype(F32)
+        cin = ic_ref[...].astype(F32).T
         c_act = (cin * sigmoid(cin)).astype(BF16)
         carried = mm(c_act, state) * erx_ref[...]
         carried_ref[...] = carried
@@ -369,8 +466,7 @@
         )
 
     def step(i, carry):
-        @pl.when(i < 8)
-        def _():
+        def take_plane():
             zz = plane_at(z, i)
 
             @pl.when(i == 0)
@@ -383,6 +479,20 @@
 
             a1(0, zz).start()
             a1(1, zz).start()
+
+            @pl.when(i < 2)
+            def _():
+                lax.fori_loop(16 * i + 8, 16 * i + 24, dispatch, 0)
+
+            @pl.when(i == 2)
+            def _():
+                lax.fori_loop(40, 48, dispatch, 0)
+
+            @pl.when(i == 3)
+            def _():
+                lax.fori_loop(48, PEERS, dispatch, 0)
+
+        pl.when((i < 8) & (i != 1))(take_plane)
 
         @pl.when((i >= 1) & (i < 9))
         def _():
@@ -392,25 +502,29 @@
             a1(1, zz).wait_recv()
             a2(1, zz).start()
 
+        pl.when(i == 1)(take_plane)
+
         @pl.when((i >= 2) & (i < 10))
         def _():
             zz = plane_at(z, i - 2)
-            a2(0, zz).wait_recv()
-            a2(1, zz).wait_recv()
 
             @pl.when(i == 2)
             def _():
-                for load in loads[:3]:
+                for load in loads[12:15]:
                     load.wait()
 
             gate = jnp.zeros((128, 256), F32)
             up = jnp.zeros((128, 256), F32)
             hgrad = jnp.zeros((128, 256), F32)
-            for q in range(NX):
+            for q in (x, left, right, far):
+                if q is far:
+                    waiter(ybuf.at[far, pl.ds(zz * 8, 8)], a2_s.at[0], a2_r.at[zz]).wait_recv()
                 rowsq = ybuf[q, pl.ds(zz * 8, 8)].reshape(128, 512)
                 gate += mm(rowsq, gw[q])
                 up += mm(rowsq, uw[q])
-                hgrad += mm(rowsq, dw[:, q * 512 : (q + 1) * 512], DIMS_NT)
+                hgrad += mm(
+                    rowsq, dw[:, pl.ds(pl.multiple_of(q * 512, 512), 512)], DIMS_NT
+                )
             gate = gate.reshape(8, 16, 256)[:, :8]
             up = up.reshape(8, 16, 256)[:, :8]
             hgrad = hgrad.reshape(8, 16, 256)[:, 8:]
@@ -452,8 +566,7 @@
         @pl.when(i >= 4)
         def _():
             zz = plane_at(z, i - 4)
-            r2(0, zz).wait_recv()
-            r2(1, zz).wait_recv()
+            waiter(rs2_r.at[:, zz], r2_s.at[0], r2_r.at[zz]).wait_recv()
             total = own_acc[zz] + rs2_r[0, zz].astype(F32) + rs2_r[1, zz].astype(F32)
             total = total.reshape(8, 8, 512)
             retbuf[pl.ds(zz * 8, 8)] = jnp.concatenate(
@@ -471,7 +584,7 @@
                 def _():
                     pltpu.make_async_remote_copy(
                         src_ref=retbuf.at[zz * 8 + m], dst_ref=backbuf.at[sp],
-                        send_sem=ret_ss.at[zz], recv_sem=ret_rs.at[z],
+                        send_sem=ret_ss.at[0], recv_sem=ret_rs.at[z],
                         device_id=peer(zz, m), device_id_type=MESH,
                     ).start()
 
@@ -485,7 +598,7 @@
 
         @pl.when(i == 2)
         def _():
-            scan_b(0, up_order)
+            scan_b()
 
         @pl.when((i >= 3) & (i < 7))
         def _():
@@ -494,7 +607,7 @@
 
         @pl.when(i == 4)
         def _():
-            scan_c(0, up_order)
+            scan_c()
 
         @pl.when(i == 7)
         def _():
@@ -502,15 +615,18 @@
             for t in range(4):
                 n1(t).start()
 
-        @pl.when(i == 10)
-        def _():
-            for t in range(1, 4):
-                n1(t).wait_recv()
-                n2(t).start()
-
         return carry
 
     lax.fori_loop(0, 12, step, 0)
+
+    outs = [
+        pltpu.make_async_copy(src, dst, o_sem.at[k])
+        for k, (src, dst) in enumerate((
+            (gout.at[0], gwg_hbm), (gout.at[1], uwg_hbm), (dout, dwg_hbm), (go_ref, go_hbm),
+            (gx_ref, gx_hbm), (gb_ref, gb_hbm), (graw_ref, graw_hbm), (gc_ref, gc_hbm),
+            (gzz_ref, gzz_hbm),
+        ))
+    ]
 
     def weights_in(q):
         g = mm(ybuf[q].reshape(1024, 512), ggi[...].reshape(1024, 512), DIMS_TN)
@@ -523,6 +639,13 @@
 
     weights_in(0)
     weights_in(1)
+    for t in range(1, 4):
+        n1(t).wait_recv()
+        n2(t).start()
+    weights_in(2)
+    weights_in(3)
+    outs[0].start()
+    outs[1].start()
 
     def arrive(k, carry):
         zz = plane_at(z, k)
@@ -548,45 +671,52 @@
     moe_grad = jnp.concatenate([mm(low, back), mm(high, back)], axis=1)
     rows[x] = (tokens_gr.astype(F32) + moe_grad).astype(BF16)
 
-    def m1(d):
-        return to_side(d, rows.at[x], rows.at[x], m_s, m_r, 0)
+    def m1(d, half):
+        blk = rows.at[x, pl.ds(64 * ((d + half) % 2), 64)]
+        return to_side(d, blk, blk, m_s.at[d, half], m_r.at[d, half])
 
     def m2(d):
         blk = rows.at[left if d == 0 else right, pl.ds(64 * d, 64)]
-        return to_side(d, blk, blk, m_s, m_r, 1)
-
-    m1(0).start()
-    m1(1).start()
-    weights_in(2)
-    m1(0).wait_recv()
-    m2(0).start()
-    m1(1).wait_recv()
-    m2(1).start()
-    weights_in(3)
+        return to_side(d, blk, blk, m_s.at[d, 2], m_r.at[d, 2])
+
+    for half in (0, 1):
+        for d in (0, 1):
+            m1(d, half).start()
+
+    own_t = rows[x].T.reshape(2, 8, 32, 128)
+    for j in range(8):
+        turned[j] = own_t[:, j]
+    tin[x, me_yc] = turned[me_yc]
+
+    def t1_go(t, carry):
+        m = lax.rem(me_yc + t, 8)
+        group_send(turned, tin.at[x], m, t1_s.at[0], t1_r.at[0]).start()
+        return carry
+
+    lax.fori_loop(1, 8, t1_go, 0)
+
+    def u1(d):
+        return to_side(d, tin.at[x], tin.at[x], u_s.at[d, 0], u_r.at[d, 0])
+
+    def u2(d):
+        blk = tin.at[left if d == 0 else right, pl.ds(4 * d, 4)]
+        return to_side(d, blk, blk, u_s.at[d, 1], u_r.at[d, 1])
+
+    loads[15].wait()
+    norm_grad = mm(rows[x], wo[x])
+    for d in (0, 1):
+        m1(d, 0).wait_recv()
+        m2(d).start()
+    seven(tin.at[x], t1_s.at[0], t1_r.at[0]).wait_recv()
+    u1(0).start()
+    u1(1).start()
+    for d in (0, 1):
+        m1(d, 1).wait_recv()
+    norm_grad += mm(rows[left], wo[left])
+    norm_grad += mm(rows[right], wo[right])
     m2(0).wait_recv()
     m2(1).wait_recv()
-
-    for q in range(NX):
-        turned[2 * q : 2 * q + 2] = rows[q].T.reshape(2, 8, 32, 128)
-    turned_in[me_yc] = turned[:, me_yc]
-
-    def t1(m):
-        return pltpu.make_async_remote_copy(
-            src_ref=turned.at[:, m], dst_ref=turned_in.at[me_yc],
-            send_sem=t1_s.at[0], recv_sem=t1_r.at[0],
-            device_id=peer(z, m), device_id_type=MESH,
-        )
-
-    def t1_go(t, carry):
-        t1(lax.rem(me_yc + t, 8)).start()
-        return carry
-
-    lax.fori_loop(1, 8, t1_go, 0)
-
-    loads[3].wait()
-    norm_grad = mm(rows[0], wo[0])
-    for q in range(1, NX):
-        norm_grad += mm(rows[q], wo[q])
+    norm_grad += mm(rows[far], wo[far])
     inv = inv_ref[:, 0:1]
     gated = gated_ref[...]
     scale = norm_grad * gain_ref[...]
@@ -595,15 +725,20 @@
     zsig = sigmoid(zin)
     dmix = dgated * (zin * zsig)
     dy_ref[...] = dmix
-    cin = ic_ref[...].astype(F32)
+    cin = ic_ref[...].astype(F32).T
     c_sig = sigmoid(cin)
     c_act = (cin * c_sig).astype(BF16)
     leaving = (dmix * erx_ref[...]).astype(BF16)
-    scan_a(1, mm(c_act, leaving, DIMS_TN), erx_ref[127:128, :])
+    back_a(mm(c_act, leaving, DIMS_TN))
+    u1(0).wait_recv()
+    u2(0).start()
+    u1(1).wait_recv()
+    u2(1).start()
     xin = ix_ref[...].astype(F32)
     xsig = sigmoid(xin)
     mixed = inside_ref[...] + carried_ref[...] + xin * xsig * skip_lanes()
     gzz_ref[...] = (dgated * mixed * (zsig * (1.0 + zin * (1.0 - zsig)))).astype(BF16)
+    outs[8].start()
     dsc_ref[...] = jnp.zeros((128, 128), F32)
 
     def pair_back(p, carry):
@@ -619,45 +754,74 @@
         return carry
 
     lax.fori_loop(0, 4, pair_back, 0)
-    scan_b(1, down_order)
     n1(0).wait_recv()
     for t in range(1, 4):
         n2(t).wait_recv()
-    seven(turned_in, t1_s.at[0], t1_r.at[0]).wait_recv()
-    terms_out = mm(turned_in[0].reshape(256, 128), nr[0])
+    u2(0).wait_recv()
+    u2(1).wait_recv()
+    terms_out = mm(tin[:, 0].reshape(256, 128), nr[0])
     for m in range(1, 8):
-        terms_out += mm(turned_in[m].reshape(256, 128), nr[m])
+        terms_out += mm(tin[:, m].reshape(256, 128), nr[m])
     part[...] = terms_out.reshape(8, 32, 1024).astype(BF16)
-    parts_in[z] = part[z]
-
-    def t2_go(t, carry):
-        zz = lax.rem(z + t, NZ)
-        plane_send(part.at[zz], parts_in, zz, t2_s.at[0], t2_r.at[0]).start()
-        return carry
-
-    lax.fori_loop(1, NZ, t2_go, 0)
+    back_b()
+
+    def at_plane(t):
+        return lax.rem(z + t + NZ, NZ)
+
+    def t2_far(d):
+        return pltpu.make_async_remote_copy(
+            src_ref=part.at[at_plane(4), pl.ds(16 * d, 16)], dst_ref=far_in.at[d],
+            send_sem=t3_s.at[d], recv_sem=t3_r.at[d],
+            device_id=peer(at_plane(1 - 2 * d), me_yc), device_id_type=MESH,
+        )
+
+    def t2(t):
+        zz = at_plane(t)
+        return plane_send(part.at[zz], parts_in, zz, t2_s.at[0], t2_r.at[0])
+
+    def six(buf, ssem, rsem):
+        blk = buf.at[pl.ds(0, 6)]
+        return pltpu.make_async_remote_copy(
+            src_ref=blk, dst_ref=blk, send_sem=ssem, recv_sem=rsem,
+            device_id={"tp": right}, device_id_type=MESH,
+        )
+
+    t2_far(0).start()
+    t2_far(1).start()
+    for t in (1, -1, 2, -2):
+        t2(t).start()
     lax.fori_loop(4, 8, pair_back, 0)
-    scan_c(1, down_order)
+    back_c()
+    t2_far(0).wait_recv()
+    over = at_plane(3)
+    part[over, 0:16] = (part[over, 0:16].astype(F32) + far_in[0].astype(F32)).astype(BF16)
+    t2(3).start()
+    t2_far(1).wait_recv()
+    under = at_plane(-3)
+    part[under, 16:32] = (part[under, 16:32].astype(F32) + far_in[1].astype(F32)).astype(BF16)
+    t2(-3).start()
     state = carry_ref[...]
     dsc = dsc_ref[...].astype(BF16)
-    bin_ = ib_ref[...].astype(F32)
+    bin_ = ib_ref[...].astype(F32).T
     b_sig = sigmoid(bin_)
     b_act = (bin_ * b_sig).astype(BF16)
     dc = mm(dsc, b_act) + mm(leaving, state, DIMS_NT)
-    gc_ref[...] = dc * (c_sig * (1.0 + cin * (1.0 - c_sig)))
+    gc_ref[...] = (dc * (c_sig * (1.0 + cin * (1.0 - c_sig)))).T
+    outs[7].start()
     e = head_map()
     dmix_b = dmix.astype(BF16).astype(F32)
     scaled = scaled_ref[...]
     scaled_b = scaled.astype(BF16).astype(F32)
     ds1 = ds1_ref[...]
     turn = per_head(dmix_b * inside_ref[...] + dmix * carried_ref[...] - scaled_b * ds1, e)
-    for q in range(2):
+    for q in range(NX):
         weights_down(q)
+    outs[2].start()
     after = scan_d(1)
     tex = tex_ref[...]
     ds2 = mm(b_act, after) * tex
     db = mm(dsc, c_act, DIMS_TN) + mm((scaled * tex).astype(BF16), after, DIMS_NT)
-    gb_ref[...] = db * (b_sig * (1.0 + bin_ * (1.0 - b_sig)))
+    gb_ref[...] = (db * (b_sig * (1.0 + bin_ * (1.0 - b_sig)))).T
     dscaled = ds1 + ds2
     gx_ref[...] = (
         (dscaled * stepx_ref[...] + dmix * skip_lanes()) * (xsig * (1.0 + xin * (1.0 - xsig)))
@@ -668,55 +832,48 @@
     at_end = jnp.sum(fade, axis=0, keepdims=True) + at_end * jnp.exp(r_ref[127:128, :])
     later = (iota((128, 128), 0) <= iota((128, 128), 1)).astype(F32).astype(BF16)
     dlog_grad = tri_sum(later, turn - fade) + at_end
-    raw = raw_ref[...]
+    raw = upright(raw_ref[...])
     dstep = per_head(dscaled * (xin * xsig), e) - dlog_grad * decay_ref[...]
-    graw_ref[...] = dstep * sigmoid(raw)
-    for q in range(2, NX):
-        weights_down(q)
-    outs = [
-        pltpu.make_async_copy(src, dst, o_sem.at[k])
-        for k, (src, dst) in enumerate(((gout.at[0], gwg_hbm), (gout.at[1], uwg_hbm), (dout, dwg_hbm)))
-    ]
-    for out in outs:
-        out.start()
-    seven(parts_in, t2_s.at[0], t2_r.at[0]).wait_recv()
-    total = parts_in[0].astype(F32)
-    for zz in range(1, NZ):
-        total += parts_in[zz].astype(F32)
-    go_ref[...] = total
-
-    def drain(k, carry):
-        @pl.when(k == z)
-        def _():
-            plane_copy(sendbuf, 7, k, disp_ss, disp_rs).wait_send()
-            plane_copy(retbuf, 7, k, ret_ss, ret_rs).wait_send()
-
-        @pl.when(k != z)
-        def _():
-            plane_copy(sendbuf, 8, k, disp_ss, disp_rs).wait_send()
-            plane_copy(retbuf, 8, k, ret_ss, ret_rs).wait_send()
-
-        for d in (0, 1):
-            a1(d, k).wait_send()
-            a2(d, k).wait_send()
-            r1(d, k).wait_send()
-            r2(d, k).wait_send()
-        return carry
-
-    lax.fori_loop(0, NZ, drain, 0)
+    graw_ref[...] = flat(dstep * sigmoid(raw))
+    for k in range(4, 7):
+        outs[k].start()
+    waiter(sendbuf.at[pl.ds(0, 63)], disp_ss.at[0], disp_rs.at[0]).wait_send()
+    waiter(retbuf.at[pl.ds(0, 63)], ret_ss.at[0], ret_rs.at[0]).wait_send()
+    waiter(ybuf.at[pl.ds(0, 2)], a1_s.at[0], a1_r.at[0, 0]).wait_send()
+    waiter(ybuf.at[0], a2_s.at[0], a2_r.at[0]).wait_send()
+    waiter(rs1_s, r1_s.at[0], r1_r.at[0, 0]).wait_send()
+    waiter(rs2_s, r2_s.at[0], r2_r.at[0]).wait_send()
     for d in (0, 1):
-        m1(d).wait_send()
+        m1(d, 0).wait_send()
+        m1(d, 1).wait_send()
         m2(d).wait_send()
-    for k in (0, 1):
-        seven(msg_a.at[k], sa_s.at[k], sa_r.at[k]).wait_send()
-        seven(rec_b.at[k], sb_s.at[k], sb_r.at[k]).wait_send()
-        seven(msg_c.at[k], sc_s.at[k], sc_r.at[k]).wait_send()
+        u1(d).wait_send()
+        u2(d).wait_send()
+    seven(msg_a, sa_s.at[0], sa_r.at[0]).wait_send()
+    seven(rec_b, sb_s.at[0], sb_r.at[0]).wait_send()
+    seven(msg_c.at[0], sc_s.at[0], sc_r.at[0]).wait_send()
+    seven(bmsg_a, sa_s.at[1], sa_r.at[1]).wait_send()
+    seven(msg_c.at[1], sc_s.at[1], sc_r.at[1]).wait_send()
+    for zz in range(NZ - 1):
+
+        @pl.when(zz < z)
+        def _():
+            back_send(zz).wait_send()
+
     for t in range(4):
         n1(t).wait_send()
     for t in range(1, 4):
         n2(t).wait_send()
-    seven(turned_in, t1_s.at[0], t1_r.at[0]).wait_send()
-    seven(part, t2_s.at[0], t2_r.at[0]).wait_send()
+    seven(turned, t1_s.at[0], t1_r.at[0]).wait_send()
+    t2_far(0).wait_send()
+    t2_far(1).wait_send()
+    six(part, t2_s.at[0], t2_r.at[0]).wait_send()
+    six(parts_in, t2_s.at[0], t2_r.at[0]).wait_recv()
+    total = part[at_plane(0)].astype(F32)
+    for t in (1, -1, 2, -2, 3, -3):
+        total += parts_in[at_plane(t)].astype(F32)
+    go_ref[...] = total
+    outs[3].start()
     for out in outs:
         out.wait()
 
@@ -725,24 +882,24 @@
     moe_input, cotangent, expert_ids, routing_weights, gate_weight, up_weight, down_weight,
     inner_x, inner_b, inner_c, gate_z, step_raw, decay_rate, skip_weight, norm_gain, w_out,
 ):
-    vmem = pl.BlockSpec(memory_space=pltpu.VMEM)
     hbm = pl.BlockSpec(memory_space=pl.ANY)
     dma = pltpu.SemaphoreType.DMA
     V = pltpu.VMEM
     S = jax.ShapeDtypeStruct
-    sems = [dma((4,)), dma((3,)), dma((8,)), dma((8,)), dma((8,)), dma((8,))]
-    sems += [dma((2, 8))] * 8 + [dma((2, 2))] * 2
+    sems = [dma((16,)), dma((9,)), dma((1,)), dma((8,)), dma((1,)), dma((8,))]
+    one, each, pairs = dma((1,)), dma((8,)), dma((2, 8))
+    sems += [one, pairs, one, each, one, pairs, one, each] + [dma((2, 3))] * 2
     wide = V((128, 1024), F32)
     go, gx, gb, gc, gzz, graw, gwg, uwg, dwg = pl.pallas_call(
         fused_kernel,
         name="fused",
         out_shape=(
-            S((32, 1024), F32), S((128, 1024), BF16), S((128, 64), F32), S((128, 64), F32),
-            S((128, 1024), BF16), S((128, 16), F32),
+            S((32, 1024), F32), S((128, 1024), BF16), S((64, 128), F32), S((64, 128), F32),
+            S((128, 1024), BF16), S((16, 128), F32),
             S((NX, 512, 256), BF16), S((NX, 512, 256), BF16), S((256, 2048), BF16),
         ),
-        in_specs=[vmem] * 12 + [hbm] * 4,
-        out_specs=(vmem,) * 6 + (hbm,) * 3,
+        in_specs=[hbm] * 16,
+        out_specs=(hbm,) * 9,
         scratch_shapes=[
             V((64, 16, 512), BF16), V((NX, 64, 16, 512), BF16),
             V((NX, 512, 256), BF16), V((NX, 512, 256), BF16), V((256, 2048), BF16),
@@ -753,30 +910,68 @@
             V((64, 16, 256), BF16), V((64, 16, 256), BF16),
             V((NX, 128, 512), BF16), V((2, NX, 512, 256), BF16), V((256, 2048), BF16),
         ] + sems + [
+            V((32, 1024), F32), V((128, 1024), BF16), V((64, 128), F32), V((64, 128), F32),
+            V((128, 1024), BF16), V((16, 128), F32),
+            V((8, 64, 128), BF16), V((8, 64, 128), BF16), V((64, 128), BF16),
+            V((8, 64, 128), BF16), V((64, 128), F32), V((2, 16, 1024), BF16),
+            dma((8,)), dma((8,)), dma((2,)), dma((2,)),
+            V((2, 128), jnp.int32), V((2, 128), F32), V((128, 512), BF16), V((128, 512), BF16),
+            V((128, 1024), BF16), V((64, 128), BF16), V((64, 128), BF16), V((128, 1024), BF16),
+            V((16, 128), F32), V((1, 16), F32), V((1, 16), F32), V((1, 1024), F32),
             V((NX, 512, 1024), BF16), wide, wide, wide, wide, V((128, 16), F32),
-            V((128, 128), F32), V((128, 128), F32), V((16, 128, 128), F32),
+            V((16, 128), F32), V((128, 128), F32), V((16, 128, 128), F32),
             V((16, 128, 128), BF16), wide, V((64, 1024), BF16), wide,
             V((8, 128, 1024), BF16), wide, V((128, 128), F32), wide, wide, V((128, 128), F32),
-            V((2, 8, 80, 128), BF16), V((2, 8, 80, 128), BF16), V((2, 80, 128), BF16),
-            V((2, 8, 80, 128), BF16), V((2, 8, 64, 128), BF16), V((2, 8, 64, 128), BF16),
-            V((2, 8, 64, 128), F32), V((2, 8, 8, 128), F32),
-            V((8, 8, 32, 128), BF16), V((8, 8, 32, 128), BF16),
+            V((8, 80, 128), BF16), V((8, 80, 128), BF16), V((80, 128), BF16),
+            V((8, 80, 128), BF16), V((2, 8, 64, 128), BF16), V((2, 8, 64, 128), BF16),
+            V((8, 64, 128), F32), V((8, 8, 128), F32),
+            V((8, 2, 32, 128), BF16), V((NX, 8, 2, 32, 128), BF16),
             V((8, 32, 1024), BF16), V((8, 32, 1024), BF16),
-        ] + [dma((2,))] * 6 + [dma((7,))] * 2 + [dma((1,))] * 4,
+        ] + [dma((2,))] * 6 + [dma((7,))] * 2 + [dma((1,))] * 4 + [dma((2, 2))] * 2,
         compiler_params=pltpu.CompilerParams(
             collective_id=0, has_side_effects=True, vmem_limit_bytes=63 * 1024 * 1024
         ),
     )(
         expert_ids.T, routing_weights.T, moe_input, cotangent,
-        inner_x, inner_b, inner_c, gate_z, step_raw,
+        inner_x, inner_b.T, inner_c.T, gate_z, step_raw.T,
         decay_rate.reshape(1, 16), skip_weight.reshape(1, 16), norm_gain.reshape(1, 1024),
         gate_weight.reshape(NX, 512, 256), up_weight.reshape(NX, 512, 256),
         down_weight.reshape(256, 2048), w_out.reshape(NX, 512, 1024),
     )
-    return (
-        gwg.reshape(1, 2048, 256), uwg.reshape(1, 2048, 256), dwg.reshape(1, 256, 2048),
-        go, gx, gb, gc, gzz, graw,
+    gwg, uwg, dwg, go, gx, gb, gc, gzz, graw = handed_over(
+        gwg.reshape(2048, 256), uwg.reshape(2048, 256), dwg, go, gx, gb, gc, gzz, graw
     )
+    return gwg[None], uwg[None], dwg[None], go, gx, gb.T, gc.T, gzz, graw.T
+
+
+def hand_over_kernel(*refs):
+    count = (len(refs) - 2) // 3
+    srcs, dsts, held = refs[:count], refs[count : 2 * count], refs[2 * count : 3 * count]
+    in_sem, out_sem = refs[3 * count :]
+    ins = [pltpu.make_async_copy(srcs[k], held[k], in_sem.at[k]) for k in range(count)]
+    outs = [pltpu.make_async_copy(held[k], dsts[k], out_sem.at[k]) for k in range(count)]
+    for k in range(count):
+        ins[k].start()
+    for k in range(count):
+        ins[k].wait()
+        outs[k].start()
+    for k in range(count):
+        outs[k].wait()
+
+
+def handed_over(*arrays):
+    hbm = pl.BlockSpec(memory_space=pl.ANY)
+    count = len(arrays)
+    return pl.pallas_call(
+        hand_over_kernel,
+        name="handover",
+        out_shape=tuple(jax.ShapeDtypeStruct(a.shape, a.dtype) for a in arrays),
+        in_specs=[hbm] * count,
+        out_specs=(hbm,) * count,
+        scratch_shapes=[pltpu.VMEM(a.shape, a.dtype) for a in arrays]
+        + [pltpu.SemaphoreType.DMA((count,))] * 2,
+        compiler_params=pltpu.CompilerParams(vmem_limit_bytes=60 * 1024 * 1024),
+    )(*arrays)
 
 
 def solution(mesh):

time: 139 us -> 114 us (0.82)
  local copies, waits for them, and re-layouts: 16.6 us -> 0 us
  Pallas kernels: 121 us -> 114 us
    unnamed x20 -> x0, local copies, waits for them, and re-layouts: 16.6 us -> none
    pallas_call x1, Pallas kernels: 121 us -> 110 us  [fused_call(): pl.pallas_call(fused_kernel, name='fused', out_shape=(S((32, 1024), F32),...]
    pallas_call x0 -> x1, Pallas kernels: none -> 3.28 us  [handed_over(): pl.pallas_call(hand_over_kernel, name='handover', out_shape=tuple((jax.Sh...]
where the time goes in v2:
time: 114 us
  Pallas kernels  114 us (100%)
    pallas_call x1, Pallas kernels, fused_call(): pl.pallas_call(fused_kernel, name='fused', out_shape=(S((32, 1024), F32),...  110 us
    pallas_call x1, Pallas kernels, handed_over(): pl.pallas_call(hand_over_kernel, name='handover', out_shape=tuple((jax.Sh...  3.28 us

profile of v2, /device:TPU:1, one launch (start us, length us, event | category | flops | bytes accessed | tf_op | source)
XLA Modules:
  0.0 114.2 jit_solution(3053296133395611006)
XLA Ops:
  0.6 110.3 %fused.1 = (f32[32,1024]{1,0:T(8,128)}, bf16[128,1024]{1,0:T(8,128)(2,1)}, f32[64,128]{1,0:T(8,128)}, f32[64,128]{1,0:T(8,128)}, bf16[128,1024]{1,0:T(8,128)(2,1...) custom-call(s32[2,128]{1,0:T(2,128)} %bitcast.30, ...), custom_call_target="tpu_custom_call" | custom-call | tf_op jit(solution)/shard_map/fused/pallas_call | solution.py:893
  111.0 3.3 %handover.1 = (bf16[2048,256]{1,0:T(8,128)(2,1)}, bf16[2048,256]{1,0:T(8,128)(2,1)}, bf16[256,2048]{1,0:T(8,128)(2,1)}, f32[32,1024]{1,0:T(8,128)}, bf16[128,102...) custom-call(bf16[2048,256]{1,0:T(8,128)(2,1)} %bitcast.21, ...), custom_call_target="tpu_custom_call" | custom-call | tf_op jit(solution)/shard_map/handover/pallas_call | solution.py:965

commit v3 on v2

--- a/solution.py
+++ b/solution.py
@@ -108,12 +108,12 @@
 def fused_kernel(
     ids_hbm, wts_hbm, min_hbm, cot_hbm, ix_hbm, ib_hbm, ic_hbm, gz_hbm, raw_hbm, decay_hbm,
     skip_hbm, gain_hbm, gw_hbm, uw_hbm, dw_hbm, wo_hbm,
-    go_hbm, gx_hbm, gb_hbm, gc_hbm, gzz_hbm, graw_hbm, gwg_hbm, uwg_hbm, dwg_hbm,
+    go_ref, gx_ref, gb_ref, gc_ref, gzz_ref, graw_ref, gwg_ref, uwg_ref, dout,
     sendbuf, ybuf, gw, uw, dw, own_acc, nbr_acc, rs1_s, rs1_r, rs2_s, rs2_r,
-    ggi, hid, retbuf, backbuf, rows, gout, dout,
-    w_sem, o_sem, disp_ss, disp_rs, ret_ss, ret_rs,
+    ggi, hid, retbuf, backbuf, rows,
+    w_sem, disp_ss, disp_rs, ret_ss, ret_rs,
     a1_s, a1_r, a2_s, a2_r, r1_s, r1_r, r2_s, r2_r, m_s, m_r,
-    go_ref, gx_ref, gb_ref, gc_ref, gzz_ref, graw_ref, bmsg_a, brec_a, bmsg_b, brec_b,
+    bmsg_a, brec_a, bmsg_b, brec_b,
     carried_back, far_in, bb_s, bb_r, t3_s, t3_r,
     ids_ref, wts_ref, min_ref, cot_ref, ix_ref, ib_ref, ic_ref, gz_ref, raw_ref, decay_ref,
     skip_ref, gain_ref, wo, scaled_ref, stepx_ref, erx_ref, tex_ref, r_ref, rt_ref, scores_ref, w_ref, m_ref,
@@ -619,19 +619,10 @@
 
     lax.fori_loop(0, 12, step, 0)
 
-    outs = [
-        pltpu.make_async_copy(src, dst, o_sem.at[k])
-        for k, (src, dst) in enumerate((
-            (gout.at[0], gwg_hbm), (gout.at[1], uwg_hbm), (dout, dwg_hbm), (go_ref, go_hbm),
-            (gx_ref, gx_hbm), (gb_ref, gb_hbm), (graw_ref, graw_hbm), (gc_ref, gc_hbm),
-            (gzz_ref, gzz_hbm),
-        ))
-    ]
-
     def weights_in(q):
         g = mm(ybuf[q].reshape(1024, 512), ggi[...].reshape(1024, 512), DIMS_TN)
-        gout[0, q] = g[:, :256].astype(BF16)
-        gout[1, q] = g[:, 256:].astype(BF16)
+        gwg_ref[q] = g[:, :256].astype(BF16)
+        uwg_ref[q] = g[:, 256:].astype(BF16)
 
     def weights_down(q):
         d = mm(hid[...].reshape(1024, 256), ybuf[q].reshape(1024, 512), DIMS_TN)
@@ -644,8 +635,6 @@
         n2(t).start()
     weights_in(2)
     weights_in(3)
-    outs[0].start()
-    outs[1].start()
 
     def arrive(k, carry):
         zz = plane_at(z, k)
@@ -695,12 +684,13 @@
 
     lax.fori_loop(1, 8, t1_go, 0)
 
-    def u1(d):
-        return to_side(d, tin.at[x], tin.at[x], u_s.at[d, 0], u_r.at[d, 0])
+    def u1(d, half):
+        blk = tin.at[x, pl.ds(4 * ((d + half) % 2), 4)]
+        return to_side(d, blk, blk, u_s.at[d, half], u_r.at[d, half])
 
     def u2(d):
         blk = tin.at[left if d == 0 else right, pl.ds(4 * d, 4)]
-        return to_side(d, blk, blk, u_s.at[d, 1], u_r.at[d, 1])
+        return to_side(d, blk, blk, u_s.at[d, 2], u_r.at[d, 2])
 
     loads[15].wait()
     norm_grad = mm(rows[x], wo[x])
@@ -708,8 +698,9 @@
         m1(d, 0).wait_recv()
         m2(d).start()
     seven(tin.at[x], t1_s.at[0], t1_r.at[0]).wait_recv()
-    u1(0).start()
-    u1(1).start()
+    for half in (0, 1):
+        for d in (0, 1):
+            u1(d, half).start()
     for d in (0, 1):
         m1(d, 1).wait_recv()
     norm_grad += mm(rows[left], wo[left])
@@ -730,15 +721,13 @@
     c_act = (cin * c_sig).astype(BF16)
     leaving = (dmix * erx_ref[...]).astype(BF16)
     back_a(mm(c_act, leaving, DIMS_TN))
-    u1(0).wait_recv()
-    u2(0).start()
-    u1(1).wait_recv()
-    u2(1).start()
+    for d in (0, 1):
+        u1(d, 0).wait_recv()
+        u2(d).start()
     xin = ix_ref[...].astype(F32)
     xsig = sigmoid(xin)
     mixed = inside_ref[...] + carried_ref[...] + xin * xsig * skip_lanes()
     gzz_ref[...] = (dgated * mixed * (zsig * (1.0 + zin * (1.0 - zsig)))).astype(BF16)
-    outs[8].start()
     dsc_ref[...] = jnp.zeros((128, 128), F32)
 
     def pair_back(p, carry):
@@ -757,6 +746,8 @@
     n1(0).wait_recv()
     for t in range(1, 4):
         n2(t).wait_recv()
+    for d in (0, 1):
+        u1(d, 1).wait_recv()
     u2(0).wait_recv()
     u2(1).wait_recv()
     terms_out = mm(tin[:, 0].reshape(256, 128), nr[0])
@@ -807,7 +798,6 @@
     b_act = (bin_ * b_sig).astype(BF16)
     dc = mm(dsc, b_act) + mm(leaving, state, DIMS_NT)
     gc_ref[...] = (dc * (c_sig * (1.0 + cin * (1.0 - c_sig)))).T
-    outs[7].start()
     e = head_map()
     dmix_b = dmix.astype(BF16).astype(F32)
     scaled = scaled_ref[...]
@@ -816,7 +806,6 @@
     turn = per_head(dmix_b * inside_ref[...] + dmix * carried_ref[...] - scaled_b * ds1, e)
     for q in range(NX):
         weights_down(q)
-    outs[2].start()
     after = scan_d(1)
     tex = tex_ref[...]
     ds2 = mm(b_act, after) * tex
@@ -835,8 +824,6 @@
     raw = upright(raw_ref[...])
     dstep = per_head(dscaled * (xin * xsig), e) - dlog_grad * decay_ref[...]
     graw_ref[...] = flat(dstep * sigmoid(raw))
-    for k in range(4, 7):
-        outs[k].start()
     waiter(sendbuf.at[pl.ds(0, 63)], disp_ss.at[0], disp_rs.at[0]).wait_send()
     waiter(retbuf.at[pl.ds(0, 63)], ret_ss.at[0], ret_rs.at[0]).wait_send()
     waiter(ybuf.at[pl.ds(0, 2)], a1_s.at[0], a1_r.at[0, 0]).wait_send()
@@ -847,7 +834,8 @@
         m1(d, 0).wait_send()
         m1(d, 1).wait_send()
         m2(d).wait_send()
-        u1(d).wait_send()
+        u1(d, 0).wait_send()
+        u1(d, 1).wait_send()
         u2(d).wait_send()
     seven(msg_a, sa_s.at[0], sa_r.at[0]).wait_send()
     seven(rec_b, sb_s.at[0], sb_r.at[0]).wait_send()
@@ -873,9 +861,6 @@
     for t in (1, -1, 2, -2, 3, -3):
         total += parts_in[at_plane(t)].astype(F32)
     go_ref[...] = total
-    outs[3].start()
-    for out in outs:
-        out.wait()
 
 
 def fused_call(
@@ -885,8 +870,8 @@
     hbm = pl.BlockSpec(memory_space=pl.ANY)
     dma = pltpu.SemaphoreType.DMA
     V = pltpu.VMEM
-    S = jax.ShapeDtypeStruct
-    sems = [dma((16,)), dma((9,)), dma((1,)), dma((8,)), dma((1,)), dma((8,))]
+    S = pltpu.VMEM
+    sems = [dma((16,)), dma((1,)), dma((8,)), dma((1,)), dma((8,))]
     one, each, pairs = dma((1,)), dma((8,)), dma((2, 8))
     sems += [one, pairs, one, each, one, pairs, one, each] + [dma((2, 3))] * 2
     wide = V((128, 1024), F32)
@@ -898,8 +883,8 @@
             S((128, 1024), BF16), S((16, 128), F32),
             S((NX, 512, 256), BF16), S((NX, 512, 256), BF16), S((256, 2048), BF16),
         ),
-        in_specs=[hbm] * 16,
-        out_specs=(hbm,) * 9,
+        in_specs=[pl.BlockSpec(memory_space=pltpu.HBM)] * 16,
+        out_specs=(pl.BlockSpec(memory_space=pltpu.VMEM),) * 9,
         scratch_shapes=[
             V((64, 16, 512), BF16), V((NX, 64, 16, 512), BF16),
             V((NX, 512, 256), BF16), V((NX, 512, 256), BF16), V((256, 2048), BF16),
@@ -908,10 +893,8 @@
             V((2, 8, 64, 512), BF16), V((2, 8, 64, 512), BF16),
             V((64, 16, 512), BF16), V((64, 16, 256), BF16),
             V((64, 16, 256), BF16), V((64, 16, 256), BF16),
-            V((NX, 128, 512), BF16), V((2, NX, 512, 256), BF16), V((256, 2048), BF16),
+            V((NX, 128, 512), BF16),
         ] + sems + [
-            V((32, 1024), F32), V((128, 1024), BF16), V((64, 128), F32), V((64, 128), F32),
-            V((128, 1024), BF16), V((16, 128), F32),
             V((8, 64, 128), BF16), V((8, 64, 128), BF16), V((64, 128), BF16),
             V((8, 64, 128), BF16), V((64, 128), F32), V((2, 16, 1024), BF16),
             dma((8,)), dma((8,)), dma((2,)), dma((2,)),
@@ -927,9 +910,9 @@
             V((8, 64, 128), F32), V((8, 8, 128), F32),
             V((8, 2, 32, 128), BF16), V((NX, 8, 2, 32, 128), BF16),
             V((8, 32, 1024), BF16), V((8, 32, 1024), BF16),
-        ] + [dma((2,))] * 6 + [dma((7,))] * 2 + [dma((1,))] * 4 + [dma((2, 2))] * 2,
+        ] + [dma((2,))] * 6 + [dma((7,))] * 2 + [dma((1,))] * 4 + [dma((2, 3))] * 2,
         compiler_params=pltpu.CompilerParams(
-            collective_id=0, has_side_effects=True, vmem_limit_bytes=63 * 1024 * 1024
+            collective_id=0, has_side_effects=True, vmem_limit_bytes=62900000
         ),
     )(
         expert_ids.T, routing_weights.T, moe_input, cotangent,
@@ -945,32 +928,25 @@
 
 
 def hand_over_kernel(*refs):
-    count = (len(refs) - 2) // 3
-    srcs, dsts, held = refs[:count], refs[count : 2 * count], refs[2 * count : 3 * count]
-    in_sem, out_sem = refs[3 * count :]
-    ins = [pltpu.make_async_copy(srcs[k], held[k], in_sem.at[k]) for k in range(count)]
-    outs = [pltpu.make_async_copy(held[k], dsts[k], out_sem.at[k]) for k in range(count)]
+    count = (len(refs) - 1) // 2
+    srcs, dsts, sem = refs[:count], refs[count : 2 * count], refs[2 * count]
+    outs = [pltpu.make_async_copy(srcs[k], dsts[k], sem.at[k]) for k in range(count)]
     for k in range(count):
-        ins[k].start()
-    for k in range(count):
-        ins[k].wait()
         outs[k].start()
     for k in range(count):
         outs[k].wait()
 
 
 def handed_over(*arrays):
-    hbm = pl.BlockSpec(memory_space=pl.ANY)
     count = len(arrays)
     return pl.pallas_call(
         hand_over_kernel,
         name="handover",
         out_shape=tuple(jax.ShapeDtypeStruct(a.shape, a.dtype) for a in arrays),
-        in_specs=[hbm] * count,
-        out_specs=(hbm,) * count,
-        scratch_shapes=[pltpu.VMEM(a.shape, a.dtype) for a in arrays]
-        + [pltpu.SemaphoreType.DMA((count,))] * 2,
-        compiler_params=pltpu.CompilerParams(vmem_limit_bytes=60 * 1024 * 1024),
+        in_specs=[pl.BlockSpec(memory_space=pltpu.VMEM)] * count,
+        out_specs=(pl.BlockSpec(memory_space=pl.ANY),) * count,
+        scratch_shapes=[pltpu.SemaphoreType.DMA((count,))],
+        compiler_params=pltpu.CompilerParams(vmem_limit_bytes=16 * 1024 * 1024),
     )(*arrays)
 
 

time: 114 us -> 113 us (level)
  Pallas kernels: 114 us -> 112 us
    pallas_call x1, Pallas kernels: 3.28 us -> 1.98 us  [handed_over(): pl.pallas_call(hand_over_kernel, name='handover', out_shape=tuple((jax.Sh...]
where the time goes in v3:
time: 113 us; the launch traced here: 112 us
  Pallas kernels  112 us (99%)
    pallas_call x1, Pallas kernels, fused_call(): pl.pallas_call(fused_kernel, name='fused', out_shape=(S((32, 1024), F32),...  110 us

profile of v3, /device:TPU:1, one launch (start us, length us, event | category | flops | bytes accessed | tf_op | source)
XLA Modules:
  0.0 112.2 jit_solution(14881983946971246836)
XLA Ops:
  0.6 109.6 %fused.1 = (f32[32,1024]{1,0:T(8,128)S(1)}, bf16[128,1024]{1,0:T(8,128)(2,1)S(1)}, f32[64,128]{1,0:T(8,128)S(1)}, f32[64,128]{1,0:T(8,128)S(1)}, bf16[128,1024]{...) custom-call(s32[2,128]{1,0:T(2,128)} %bitcast.30, ...), custom_call_target="tpu_custom_call" | custom-call | tf_op jit(solution)/shard_map/fused/pallas_call | solution.py:878
  110.2 2.0 %handover.1 = (bf16[2048,256]{1,0:T(8,128)(2,1)}, bf16[2048,256]{1,0:T(8,128)(2,1)}, bf16[256,2048]{1,0:T(8,128)(2,1)}, f32[32,1024]{1,0:T(8,128)}, bf16[128,102...) custom-call(bf16[2048,256]{1,0:T(8,128)(2,1)S(1)} %bitcast.20, ...), custom_call_target="tpu_custom_call" | custom-call | tf_op jit(solution)/shard_map/handover/pallas_call | solution.py:942

commit v4 on v3

--- a/solution.py
+++ b/solution.py
@@ -261,7 +261,7 @@
         rec_a[me_yc] = msg_a[me_yc]
 
         def go(t, carry):
-            m = lax.rem(me_yc + t, 8)
+            m = lax.rem(me_yc + lax.rem(t + 1, 7) + 1, 8)
             group_send(msg_a, rec_a, m, sa_s.at[0], sa_r.at[0]).start()
             return carry
 
@@ -300,7 +300,7 @@
         rec_c[0, me_yc] = msg_c[0, me_yc]
 
         def go(t, carry):
-            m = lax.rem(me_yc + t, 8)
+            m = lax.rem(me_yc + lax.rem(t + 1, 7) + 1, 8)
             group_send(msg_c.at[0], rec_c.at[0], m, sc_s.at[0], sc_r.at[0]).start()
             return carry
 
@@ -324,7 +324,7 @@
         brec_a[me_yc] = bmsg_a[me_yc]
 
         def go(t, carry):
-            m = lax.rem(me_yc + t, 8)
+            m = lax.rem(me_yc + lax.rem(t + 1, 7) + 1, 8)
             group_send(bmsg_a, brec_a, m, sa_s.at[1], sa_r.at[1]).start()
             return carry
 
@@ -376,7 +376,7 @@
         rec_c[1, me_yc] = msg_c[1, me_yc]
 
         def go(t, carry):
-            m = lax.rem(me_yc + t, 8)
+            m = lax.rem(me_yc + lax.rem(t + 1, 7) + 1, 8)
             group_send(msg_c.at[1], rec_c.at[1], m, sc_s.at[1], sc_r.at[1]).start()
             return carry
 
@@ -678,7 +678,7 @@
     tin[x, me_yc] = turned[me_yc]
 
     def t1_go(t, carry):
-        m = lax.rem(me_yc + t, 8)
+        m = lax.rem(me_yc + lax.rem(t + 1, 7) + 1, 8)
         group_send(turned, tin.at[x], m, t1_s.at[0], t1_r.at[0]).start()
         return carry
 

time: 113 us -> 113 us (level)
  no operation moved by 1% of the time
where the time goes in v4:
time: 113 us
  Pallas kernels  113 us (100%)
    pallas_call x1, Pallas kernels, fused_call(): pl.pallas_call(fused_kernel, name='fused', out_shape=(S((32, 1024), F32),...  111 us

profile of v4, /device:TPU:1, one launch (start us, length us, event | category | flops | bytes accessed | tf_op | source)
XLA Modules:
  0.0 113.2 jit_solution(8400940045335759460)
XLA Ops:
  0.6 110.6 %fused.1 = (f32[32,1024]{1,0:T(8,128)S(1)}, bf16[128,1024]{1,0:T(8,128)(2,1)S(1)}, f32[64,128]{1,0:T(8,128)S(1)}, f32[64,128]{1,0:T(8,128)S(1)}, bf16[128,1024]{...) custom-call(s32[2,128]{1,0:T(2,128)} %bitcast.30, ...), custom_call_target="tpu_custom_call" | custom-call | tf_op jit(solution)/shard_map/fused/pallas_call | solution.py:878
  111.2 2.0 %handover.1 = (bf16[2048,256]{1,0:T(8,128)(2,1)}, bf16[2048,256]{1,0:T(8,128)(2,1)}, bf16[256,2048]{1,0:T(8,128)(2,1)}, f32[32,1024]{1,0:T(8,128)}, bf16[128,102...) custom-call(bf16[2048,256]{1,0:T(8,128)(2,1)S(1)} %bitcast.20, ...), custom_call_target="tpu_custom_call" | custom-call | tf_op jit(solution)/shard_map/handover/pallas_call | solution.py:942
